TPU v7x, 32 devices: a whole 2x2x4 slice. The times are simulated.
32 devices in a mesh: sp: 8 (over z, x), tp: 4 (over y, core).
Axes of the slice: x: 2, y: 2, z: 4, core: 2. Of those that a mesh axis runs over, the one named last changes fastest.
Arguments:
- mixer_input: bfloat16 [4096, 2048], P('sp', 'tp'), may hold values from -6 to 6
- residual: bfloat16 [4096, 2048], P(('sp', 'tp')), may hold values from -6 to 6
- log_step: float32 [128], P('tp'), may hold values from -3.9 to -2.3
- rate_real: float32 [128, 64], P('tp'), may hold values from -1.5 to 0, as said below
- rate_imag: float32 [128, 64], P('tp'), may hold values from 2 to 30
- damping: float32 [4096, 128], P('sp', 'tp'), may hold values from -2 to 0, as said below
- in_map: float32 [2, 128, 64, 16], P(None, 'tp'), may hold values from -1 to 1
- out_map: float32 [2, 128, 16, 64], P(None, 'tp'), may hold values from -0.75 to 0.75
- skip: float32 [2048], P('tp'), may hold values from -3 to 3
- w_out: bfloat16 [2048, 2048], P('tp'), may hold values from -0.125 to 0.125
- norm_gain: float32 [2048], replicated, may hold values from 0.1 to 1.9
- w_act: bfloat16 [2048, 5632], P('sp', 'tp'), may hold values from -0.125 to 0.125
- w_lin: bfloat16 [2048, 5632], P('sp', 'tp'), may hold values from -0.125 to 0.125
- conv_taps: float32 [2, 3, 5632], P(None, None, 'tp'), may hold values from -3.5 to 3.5
- w_down: bfloat16 [5632, 2048], P('tp', 'sp'), may hold values from -0.078125 to 0.078125
Outputs:
- layer_out: bfloat16 [4096, 2048], P(('sp', 'tp'))
Inputs may be any that keep to these rules, and one draw needn't show every extreme that they name: `rate_real`: all entries negative. `damping`: all entries at most zero.
All inputs are finite; a program needn't handle non-finite values.
Results may differ from a plain program's by a relative error of at most 0.02.
Values may be sent and summed in bfloat16 or wider, within the bound.
A program may use at most 192 MiB of HBM per device.

v0:
```python
import jax
import jax.numpy as jnp
from jax import lax
from jax.sharding import PartitionSpec as P

CONV = 3


def entering(value, axis, join, neutral):
    count, mine = (lax.axis_size(axis), lax.axis_index(axis))
    pieces = jax.tree.map(lambda part: lax.all_gather(part, axis), value)
    total = jax.tree.map(
        lambda part, zero: jnp.full_like(part, 0) + jnp.asarray(zero, part.dtype), value, neutral
    )

    def step(position, total):
        longer = join(total, jax.tree.map(lambda part: part[position], pieces))
        return jax.tree.map(lambda new, old: jnp.where(position < mine, new, old), longer, total)

    return lax.fori_loop(0, count - 1, step, total)


def from_partner(block, axis, apart):
    count = lax.axis_size(axis)
    route = []
    for low in range(count):
        high = low | 1 << apart
        if high != low and high < count:
            route += [(low, high), (high, low)]
    return lax.ppermute(block, axis, route)


def from_behind(value, axis, steps):
    count = lax.axis_size(axis)
    initial, last = (max(0, -steps), min(count, count - steps))
    return lax.ppermute(value, axis, [(source, source + steps) for source in range(initial, last)])


def combine(earlier, later):
    a1r, a1i, b1r, b1i = earlier
    a2r, a2i, b2r, b2i = later
    return (
        a2r * a1r - a2i * a1i,
        a2r * a1i + a2i * a1r,
        a2r * b1r - a2i * b1i + b2r,
        a2r * b1i + a2i * b1r + b2i,
    )


def advance(carry, item):
    start_re, start_im, before_re, before_im = carry
    trans_re, trans_im, end_re, end_im = item
    new_carry = (
        trans_re * start_re - trans_im * start_im + end_re,
        trans_re * start_im + trans_im * start_re + end_im,
        trans_re * before_re - trans_im * before_im,
        trans_re * before_im + trans_im * before_re,
    )
    return (new_carry, carry)


def state_mixer(mixer_input, log_step, rate_real, rate_imag, damping, in_map, out_map, skip):
    highest = lax.Precision.HIGHEST
    tokens_here, channels = mixer_input.shape
    groups_here, states = rate_real.shape
    group_width = channels // groups_here
    step_size = jnp.exp(log_step)[:, None]
    log_rate = rate_real * step_size
    angle_step = rate_imag * step_size
    magnitude = jnp.exp(log_rate)
    abar_re = magnitude * jnp.cos(angle_step)
    abar_im = magnitude * jnp.sin(angle_step)
    denominator = rate_real * rate_real + rate_imag * rate_imag
    minus_one = abar_re - 1.0
    factor_re = (minus_one * rate_real + abar_im * rate_imag) / denominator
    factor_im = (abar_im * rate_real - minus_one * rate_imag) / denominator
    bbar_re = factor_re[..., None] * in_map[0] - factor_im[..., None] * in_map[1]
    bbar_im = factor_re[..., None] * in_map[1] + factor_im[..., None] * in_map[0]
    block_len = min(32, tokens_here)
    block_count = tokens_here // block_len
    inputs = mixer_input.astype(jnp.float32).reshape(
        block_count, block_len, groups_here, group_width
    )
    drive_re = jnp.einsum("bkgh,gph->bkgp", inputs, bbar_re, precision=highest)
    drive_im = jnp.einsum("bkgh,gph->bkgp", inputs, bbar_im, precision=highest)
    damp_cum = jnp.cumsum(damping.reshape(block_count, block_len, groups_here), axis=1)
    counter = jnp.arange(1, block_len + 1, dtype=jnp.float32)
    log_prefix = counter[None, :, None, None] * log_rate[None, None] + damp_cum[..., None]
    turned = counter[:, None, None] * angle_step[None]
    cosine = jnp.cos(turned)[None]
    sine = jnp.sin(turned)[None]
    growth = jnp.exp(log_prefix)
    prefix_re = growth * cosine
    prefix_im = growth * sine
    inverse = jnp.exp(-log_prefix)
    scaled_re = inverse * (drive_re * cosine + drive_im * sine)
    scaled_im = inverse * (drive_im * cosine - drive_re * sine)
    lower_ones = (jnp.arange(block_len)[:, None] >= jnp.arange(block_len)[None, :]).astype(
        jnp.float32
    )
    summed_re = jnp.einsum("kl,blgp->bkgp", lower_ones, scaled_re, precision=highest)
    summed_im = jnp.einsum("kl,blgp->bkgp", lower_ones, scaled_im, precision=highest)
    local_re = prefix_re * summed_re - prefix_im * summed_im
    local_im = prefix_re * summed_im + prefix_im * summed_re
    zeros = jnp.zeros((groups_here, states), jnp.float32)
    ones = jnp.ones((groups_here, states), jnp.float32)
    items = (prefix_re[:, -1], prefix_im[:, -1], local_re[:, -1], local_im[:, -1])
    final, starts = lax.scan(advance, (zeros, zeros, ones, zeros), items)
    incoming = entering(
        (final[2], final[3], final[0], final[1]), "sp", combine, (ones, zeros, zeros, zeros)
    )
    enter_re, enter_im = (incoming[2], incoming[3])
    begin_re = starts[0] + starts[2] * enter_re - starts[3] * enter_im
    begin_im = starts[1] + starts[2] * enter_im + starts[3] * enter_re
    state_re = local_re + prefix_re * begin_re[:, None] - prefix_im * begin_im[:, None]
    state_im = local_im + prefix_re * begin_im[:, None] + prefix_im * begin_re[:, None]
    mixed = (
        jnp.einsum("bkgp,ghp->bkgh", state_re, out_map[0], precision=highest)
        - jnp.einsum("bkgp,ghp->bkgh", state_im, out_map[1], precision=highest)
        + skip.reshape(groups_here, group_width) * inputs
    )
    return mixed.reshape(tokens_here, channels)


def normalize(stream, norm_gain):
    stream_f = stream.astype(jnp.float32)
    scale = lax.rsqrt(jnp.mean(stream_f * stream_f, axis=-1, keepdims=True) + 1e-06)
    return (stream_f * scale * norm_gain).astype(jnp.bfloat16)


def causal_conv(act_pre, lin_pre, previous, taps):
    row_count, width = act_pre.shape
    act_pad = jnp.concatenate([previous[0], act_pre], axis=0).astype(jnp.float32)
    lin_pad = jnp.concatenate([previous[1], lin_pre], axis=0).astype(jnp.float32)
    act_conv = jnp.zeros((row_count, width), jnp.float32)
    lin_conv = jnp.zeros((row_count, width), jnp.float32)
    for offset in range(CONV):
        act_conv = act_conv + taps[0, offset][None, :] * act_pad[offset : offset + row_count]
        lin_conv = lin_conv + taps[1, offset][None, :] * lin_pad[offset : offset + row_count]
    return (jax.nn.silu(act_conv) * lin_conv).astype(jnp.bfloat16)


def per_device(
    mixer_input,
    residual,
    log_step,
    rate_real,
    rate_imag,
    damping,
    in_map,
    out_map,
    skip,
    w_out,
    norm_gain,
    w_act,
    w_lin,
    conv_taps,
    w_down,
):
    tokens_here = mixer_input.shape[0]
    hidden_here = w_act.shape[1]
    mixed = state_mixer(mixer_input, log_step, rate_real, rate_imag, damping, in_map, out_map, skip)
    activated = jax.nn.gelu(mixed).astype(jnp.bfloat16)
    projected = lax.psum_scatter(
        jnp.dot(activated, w_out, preferred_element_type=jnp.float32).astype(jnp.bfloat16),
        "tp",
        scatter_dimension=0,
        tiled=True,
    ).astype(jnp.float32)
    stream = (residual.astype(jnp.float32) + projected).astype(jnp.bfloat16)
    normed_all = lax.all_gather(normalize(stream, norm_gain), "tp", axis=0, tiled=True)
    parity = lax.axis_index("sp") % 2
    half = hidden_here // 2
    copies = lax.axis_size("sp") // 2

    def outgoing_rows(weight):
        paired = jnp.concatenate([weight[:, :half], weight[:, half:]], axis=0)
        return jnp.tile(paired, (copies, 1))

    act_half, lin_half = (
        lax.all_to_all(outgoing_rows(w_act), "sp", split_axis=0, concat_axis=0, tiled=True),
        lax.all_to_all(outgoing_rows(w_lin), "sp", split_axis=0, concat_axis=0, tiled=True),
    )
    paired_down = jnp.concatenate([w_down[:half], w_down[half:]], axis=1)
    down_half = lax.all_to_all(
        jnp.tile(paired_down, (1, copies)), "sp", split_axis=1, concat_axis=1, tiled=True
    )
    partner = from_partner(normed_all, "sp", 0)
    first = jnp.where(parity == 0, normed_all, partner)
    second = jnp.where(parity == 0, partner, normed_all)
    normed_pair = jnp.concatenate([first, second], axis=0)
    act_pre = jnp.dot(normed_pair, act_half, preferred_element_type=jnp.float32).astype(
        jnp.bfloat16
    )
    lin_pre = jnp.dot(normed_pair, lin_half, preferred_element_type=jnp.float32).astype(
        jnp.bfloat16
    )
    edge = 2 * tokens_here - (CONV - 1)
    previous = from_behind((act_pre[edge:], lin_pre[edge:]), "sp", 2)
    taps = lax.dynamic_slice_in_dim(conv_taps, parity * half, half, 2)
    hidden = causal_conv(act_pre, lin_pre, previous, taps)
    partial_value = jnp.dot(hidden, down_half, preferred_element_type=jnp.float32)
    mine = lax.dynamic_slice_in_dim(partial_value, parity * tokens_here, tokens_here, 0)
    other = lax.dynamic_slice_in_dim(partial_value, (1 - parity) * tokens_here, tokens_here, 0)
    block_total = mine + from_partner(other, "sp", 0)
    channel_sum = lax.psum_scatter(
        block_total.astype(jnp.bfloat16), "tp", scatter_dimension=0, tiled=True
    ).astype(jnp.float32)
    return (stream.astype(jnp.float32) + channel_sum).astype(jnp.bfloat16)


def solution(mesh):
    in_specs = (
        P("sp", "tp"),
        P(("sp", "tp"), None),
        P("tp"),
        P("tp", None),
        P("tp", None),
        P("sp", "tp"),
        P(None, "tp", None, None),
        P(None, "tp", None, None),
        P("tp"),
        P("tp", None),
        P(),
        P("sp", "tp"),
        P("sp", "tp"),
        P(None, None, "tp"),
        P("tp", "sp"),
    )
    out_specs = P(("sp", "tp"), None)
    return jax.shard_map(
        per_device, mesh=mesh, in_specs=in_specs, out_specs=out_specs, check_vma=False
    )
```

profile of v0, /device:TPU:0, one launch (start us, length us, event | category | flops | bytes accessed | tf_op | source)
XLA Modules:
  0.0 655.9 jit_solution(3268502077172165253)
XLA Ops:
  12.6 5.7 all_to_all.24
  18.4 4.0 copy.80
  22.4 7.4 %all-to-all-start = ((bf16[8,256,704]{1,2,0:T(8,128)(2,1)}), bf16[8,256,704]{1,2,0:T(8,128)(2,1)}, u32[]{:S(2)}, u32[]{:S(2)}) async-start(bf16[8,256,704]{1,2,0:T(8,128)(2,1)} %copy.80), calls=%async_computation.1 | async-start | bytes 5767168 | tf_op jit(solution)/shard_map/all_to_all | solution.py:181
  32.9 7.4 %fusion.69 = f32[32,64,16,32]{1,3,2,0:T(8,128)} fusion(bf16[16,32,32,16]{1,0,3,2:T(8,128)(2,1)} %reshape.77, f32[2,32,64,16]{2,3,1,0:T(8,128)} %param.25, f32[32,64]{1,0:T(8,128)S(1)} %get-tuple-element.429, f32[32,64]{1,0:T(8,128)S(1)} %get-tuple-element.428), kind=kOutput, calls=%fused_computation.97 | convolution fusion | flops 201424896 | bytes 4997120 | tf_op jit(solution)/shard_map/bkgh,gph->bkgp/dot_general | solution.py:85
  40.3 5.8 fusion.71
  50.6 13.4 %fusion.29 = f32[16,32,64,32]{2,3,0,1:T(8,128)} fusion(f32[32,64,16,32]{1,3,2,0:T(8,128)} %fusion.69, f32[32,64,16,32]{1,3,2,0:T(8,128)} %fusion.71, f32[32,32,64]{2,0,1:T(8,128)S(1)} %get-tuple-element.433, f32[32,32,64]{2,0,1:T(8,128)S(1)} %get-tuple-element.432, f32[16,32,32]{1,0,2:T(8,128)S(1)} %copy.63, f32[32,32,64]{2,0,1:T(8,128)S(1)} %get-tuple-element.434), kind=kOutput, calls=%fused_computation.45 | convolution fusion | flops 408945664 | bytes 13434880 | tf_op jit(solution)/shard_map/kl,blgp->bkgp/dot_general | solution.py:101
  64.0 20.1 %fusion.15 = (f32[16,32,32,64]{3,1,0,2:T(8,128)}, f32[16,32,32,64]{3,1,0,2:T(8,128)}, f32[16,32,32,64]{3,1,0,2:T(8,128)}, f32[16,32,32,64]{3,1,0,2:T(8,128)}) fusion(f32[16,32,64,32]{2,3,0,1:T(8,128)} %fusion.29, f32[32,32,64]{2,0,1:T(8,128)S(1)} %get-tuple-element.433, f32[32,32,64]{2,0,1:T(8,128)S(1)} %get-tuple-element.432, f32[16,32,32]{1,0,2:T(8,128)S(1)} %copy.63, ...), kind=kOutput, calls=%fused_computation.35 | convolution fusion | flops 418382848 | bytes 30212096 | tf_op jit(solution)/shard_map/kl,blgp->bkgp/dot_general | solution.py:102
  94.3 52.4 %while.41 = (s32[]{:T(128)}, f32[32,64]{1,0:T(8,128)S(1)}, f32[32,64]{1,0:T(8,128)S(1)}, f32[32,64]{1,0:T(8,128)S(1)}, f32[32,64]{1,0:T(8,128)S(1)}, /*index=5*/...) while((s32[]{:T(128)}, f32[32,64]{1,0:T(8,128)S(1)}, ...), condition=%wide.region_2.3_spmd.clone, body=%wide.region_1.2_spmd.clone.sunk | while | flops 45059 | bytes 263329 | solution.py:108
  146.7 33.1 %all-gather = f32[256,64]{1,0:T(8,128)} all-gather(f32[32,64]{1,0:T(8,128)S(1)} %get-tuple-element.221), channel_id=2, replica_groups=mesh['sp'=8,'tp'=4] {'sp'}, dimensions={0}, use_global_device_ids=true | all-gather | bytes 73728 | tf_op jit(solution)/shard_map/all_gather | solution.py:11
  179.8 32.5 %all-gather.1 = f32[256,64]{1,0:T(8,128)} all-gather(f32[32,64]{1,0:T(8,128)S(1)} %get-tuple-element.222), channel_id=3, replica_groups=mesh['sp'=8,'tp'=4] {'sp'}, dimensions={0}, use_global_device_ids=true | all-gather | bytes 73728 | tf_op jit(solution)/shard_map/all_gather | solution.py:11
  212.3 32.5 %all-gather.2 = f32[256,64]{1,0:T(8,128)} all-gather(f32[32,64]{1,0:T(8,128)S(1)} %get-tuple-element.223), channel_id=4, replica_groups=mesh['sp'=8,'tp'=4] {'sp'}, dimensions={0}, use_global_device_ids=true | all-gather | bytes 73728 | tf_op jit(solution)/shard_map/all_gather | solution.py:11
  244.9 32.5 %all-gather.3 = f32[256,64]{1,0:T(8,128)} all-gather(f32[32,64]{1,0:T(8,128)S(1)} %get-tuple-element.224), channel_id=5, replica_groups=mesh['sp'=8,'tp'=4] {'sp'}, dimensions={0}, use_global_device_ids=true | all-gather | bytes 73728 | tf_op jit(solution)/shard_map/all_gather | solution.py:11
  277.4 5.7 while.42
  286.2 35.1 %fusion.17 = f32[32,16,32,16]{2,3,1,0:T(8,128)S(1)} fusion(f32[16,32,32,64]{3,1,0,2:T(8,128)} %get-tuple-element.415, f32[16,32,64]{2,0,1:T(8,128)} %copy.76, f32[16,32,64]{2,0,1:T(8,128)} %copy.75, f32[32,32,64]{2,0,1:T(8,128)S(1)} %get-tuple-element.433, f32[32,32,64]{2,0,1:T(8,128)S(1)} %get-tuple-element.432, f32[16,32,32]{1,0,2:T(8,128)S(1)} %copy.63, ...), kind=kOutput, calls=%fused_computation.37 | convolution fusion | flops 208666624 | bytes 11337728 | tf_op jit(solution)/shard_map/bkgp,ghp->bkgh/dot_general | solution.py:118
  321.3 35.4 %bitcast_add_fusion.2 = f32[16,32,32,16]{1,3,0,2:T(8,128)S(1)} fusion(f32[32,16,32,16]{2,3,1,0:T(8,128)S(1)} %fusion.17, f32[32,16]{1,0:T(8,128)S(1)} %mul.444, f32[16,32,32,64]{3,1,0,2:T(8,128)} %get-tuple-element.414, f32[16,32,64]{2,0,1:T(8,128)S(1)} %copy-done.16, f32[16,32,64]{2,0,1:T(8,128)S(1)} %copy-done.15, ...), kind=kOutput, calls=%fused_computation.54 | convolution fusion | flops 209715200 | bytes 14172160 | tf_op jit(solution)/shard_map/bkgp,ghp->bkgh/dot_general | solution.py:119
  360.4 3.8 reshape.79
  370.9 5.9 all_to_all.27
  376.8 4.1 copy.83
  380.9 5.7 all-to-all-start.1
  386.6 12.6 %reduce-scatter.3.cloned.1.call-done = bf16[128,2048]{1,0:T(8,128)(2,1)} async-done(((bf16[512,2048]{1,0:T(8,128)(2,1)}), bf16[128,2048]{1,0:T(8,128)(2,1)}) %reduce-scatter.3.cloned.1.call-update) | async-done | bytes 524304 | tf_op jit(solution)/shard_map/reduce_scatter | solution.py:164
  405.1 5.8 all_to_all.30
  411.0 4.0 copy.85
  415.0 14.1 %all-to-all-done.1 = bf16[8,256,704]{1,2,0:T(8,128)(2,1)} async-done(((bf16[8,256,704]{1,2,0:T(8,128)(2,1)}), bf16[8,256,704]{1,2,0:T(8,128)(2,1)}, u32[]{:S(2)}, u32[]{:S(2)}) %all-to-all-start.1) | async-done | bytes 2883616 | tf_op jit(solution)/shard_map/all_to_all | solution.py:182
  429.1 15.0 %all-to-all-start.2 = ((bf16[704,8,256]{2,0,1:T(8,128)(2,1)}), bf16[704,8,256]{2,0,1:T(8,128)(2,1)}, u32[]{:S(2)}, u32[]{:S(2)}) async-start(bf16[704,8,256]{2,0,1:T(8,128)(2,1)} %copy.85), calls=%async_computation.3 | async-start | bytes 5767168 | tf_op jit(solution)/shard_map/all_to_all | solution.py:185
  446.3 3.8 copy.99
  450.0 3.8 copy.100
  453.8 34.6 %all-to-all-done.2 = bf16[704,8,256]{2,0,1:T(8,128)(2,1)} async-done(((bf16[704,8,256]{2,0,1:T(8,128)(2,1)}), bf16[704,8,256]{2,0,1:T(8,128)(2,1)}, u32[]{:S(2)}, u32[]{:S(2)}) %all-to-all-start.2) | async-done | bytes 2883616 | tf_op jit(solution)/shard_map/all_to_all | solution.py:185
  490.7 9.3 %collective-permute-done = bf16[512,2048]{1,0:T(8,128)(2,1)} collective-permute-done((bf16[512,2048]{1,0:T(8,128)(2,1)}, bf16[512,2048]{1,0:T(8,128)(2,1)}, u32[]{:S(2)}, u32[]{:S(2)}) %collective-permute-start) | collective-permute-done | bytes 2097184 | tf_op jit(solution)/shard_map/ppermute | solution.py:30
  518.4 6.8 %fusion.73 = f32[1024,2048]{1,0:T(8,128)S(1)} fusion(bf16[704,2048]{1,0:T(8,128)(2,1)S(1)} %bitcast.183, f32[1026,704]{0,1:T(8,128)S(1)} %maximum_convert_fusion.1, f32[1026,704]{0,1:T(8,128)S(1)} %maximum_convert_fusion, f32[704]{0:T(1024)S(1)} %get-tuple-element.355, f32[704]{0:T(1024)S(1)} %get-tuple-element.351, f32[704]{0:T(1024)S(1)} %get-tuple-element.352, ...), kind=kOutput, calls=%fused_computation.105 | convolution fusion | flops 2964324352 | bytes 28598272 | tf_op jit(solution)/shard_map/dot_general | solution.py:202
  530.3 76.9 %collective-permute-done.3 = f32[512,2048]{1,0:T(8,128)} collective-permute-done((f32[512,2048]{1,0:T(8,128)}, f32[512,2048]{1,0:T(8,128)}, u32[]{:S(2)}, u32[]{:S(2)}) %collective-permute-start.3) | collective-permute-done | bytes 4194336 | tf_op jit(solution)/shard_map/ppermute | solution.py:30
  607.2 5.5 add_convert_fusion
  612.8 34.1 %reduce-scatter.5.cloned.1.call-done = bf16[128,2048]{1,0:T(8,128)(2,1)} async-done(((bf16[512,2048]{1,0:T(8,128)(2,1)}), bf16[128,2048]{1,0:T(8,128)(2,1)}) %reduce-scatter.5.cloned.1.call-update) | async-done | bytes 524304 | tf_op jit(solution)/shard_map/reduce_scatter | solution.py:206
  (211 shorter events, 130.3 us)
Async XLA Ops:
  6.5 357.7 %copy-start = (bf16[512,2048]{1,0:T(8,128)(2,1)S(1)}, bf16[512,2048]{1,0:T(8,128)(2,1)}, u32[]{:S(2)}) copy-start(bf16[512,2048]{1,0:T(8,128)(2,1)} %param.28) | copy-start | bytes 6291460
  22.4 7.5 %copy-start.24 = (f32[32]{0:T(128)S(1)}, f32[32]{0:T(128)}, u32[]{:S(2)}) copy-start(f32[32]{0:T(128)} %param.21) | copy-start | bytes 388
  22.4 7.5 %copy-start.13 = (bf16[512,512]{1,0:T(8,128)(2,1)S(1)}, bf16[512,512]{1,0:T(8,128)(2,1)}, u32[]{:S(2)}) copy-start(bf16[512,512]{1,0:T(8,128)(2,1)} %param.19) | copy-start | bytes 1572868
  22.4 10.4 %copy-start.18 = (f32[32,64]{1,0:T(8,128)S(1)}, f32[32,64]{1,0:T(8,128)}, u32[]{:S(2)}) copy-start(f32[32,64]{1,0:T(8,128)} %param.23) | copy-start | bytes 24580
  22.4 10.4 %copy-start.19 = (f32[32,64]{1,0:T(8,128)S(1)}, f32[32,64]{1,0:T(8,128)}, u32[]{:S(2)}) copy-start(f32[32,64]{1,0:T(8,128)} %param.22) | copy-start | bytes 24580
  22.4 358.5 %all-to-all-start = ((bf16[8,256,704]{1,2,0:T(8,128)(2,1)}), bf16[8,256,704]{1,2,0:T(8,128)(2,1)}, u32[]{:S(2)}, u32[]{:S(2)}) async-start(bf16[8,256,704]{1,2,0:T(8,128)(2,1)} %copy.80), calls=%async_computation.1 | async-start | bytes 5767168 | tf_op jit(solution)/shard_map/all_to_all | solution.py:181
  29.8 369.5 %reduce-scatter.3.cloned.1.call-start = ((), (), s32[]{:S(2)}) async-start(), calls=%async_computation.5 | async-start | bytes 2621440 | tf_op jit(solution)/shard_map/reduce_scatter | solution.py:164
  48.6 15.3 %slice-start = ((s8[8388608]{0:T(1024)(128)(4,1)}), s8[4194304]{0:T(1024)(128)(4,1)S(1)}, s32[]{:S(2)}) async-start(s8[8388608]{0:T(1024)(128)(4,1)} %bitcast.181), calls=%async_computation.8 | async-start | bytes 8388608
  50.6 13.4 %copy-start.7 = (f32[32,32,64]{2,0,1:T(8,128)}, f32[32,32,64]{2,0,1:T(8,128)S(1)}, u32[]{:S(2)}) copy-start(f32[32,32,64]{2,0,1:T(8,128)S(1)} %get-tuple-element.434) | copy-start | bytes 786436
  50.6 13.4 %slice-start.1 = ((s8[8388608]{0:T(1024)(128)(4,1)}), s8[4194304]{0:T(1024)(128)(4,1)S(1)}, s32[]{:S(2)}) async-start(s8[8388608]{0:T(1024)(128)(4,1)} %bitcast.181), calls=%async_computation.9 | async-start | bytes 8388608
  86.6 199.4 %copy-start.22 = (f32[512]{0:T(512)S(1)}, f32[512]{0:T(512)}, u32[]{:S(2)}) copy-start(f32[512]{0:T(512)} %param.27) | copy-start | bytes 6148
  286.1 35.2 %copy-start.3 = (bf16[16,32,32,16]{1,0,3,2:T(8,128)(2,1)S(1)}, bf16[16,32,32,16]{1,0,3,2:T(8,128)(2,1)}, u32[]{:S(2)}) copy-start(bf16[16,32,32,16]{1,0,3,2:T(8,128)(2,1)} %reshape.77) | copy-start | bytes 1572868
  286.1 35.2 %copy-start.8 = (f32[32,32,64]{2,0,1:T(8,128)S(1)}, f32[32,32,64]{2,0,1:T(8,128)}, u32[]{:S(2)}) copy-start(f32[32,32,64]{2,0,1:T(8,128)} %copy-done.7) | copy-start | bytes 786436
  286.2 35.2 %copy-start.15 = (f32[16,32,64]{2,0,1:T(8,128)S(1)}, f32[16,32,64]{2,0,1:T(8,128)}, u32[]{:S(2)}) copy-start(f32[16,32,64]{2,0,1:T(8,128)} %copy.75) | copy-start | bytes 393220
  286.2 35.2 %copy-start.16 = (f32[16,32,64]{2,0,1:T(8,128)S(1)}, f32[16,32,64]{2,0,1:T(8,128)}, u32[]{:S(2)}) copy-start(f32[16,32,64]{2,0,1:T(8,128)} %copy.76) | copy-start | bytes 393220
  286.2 35.2 %copy-start.23 = (f32[2,32,16,64]{3,2,1,0:T(8,128)S(1)}, f32[2,32,16,64]{3,2,1,0:T(8,128)}, u32[]{:S(2)}) copy-start(f32[2,32,16,64]{3,2,1,0:T(8,128)} %param.26) | copy-start | bytes 786436
  380.9 18.4 %copy-start.5 = (bf16[128,2048]{1,0:T(8,128)(2,1)S(1)}, bf16[128,2048]{1,0:T(8,128)(2,1)}, u32[]{:S(2)}) copy-start(bf16[128,2048]{1,0:T(8,128)(2,1)} %param.20) | copy-start | bytes 1572868
  380.9 19.7 %copy-start.21 = (f32[2048]{0:T(1024)S(1)}, f32[2048]{0:T(1024)}, u32[]{:S(2)}) copy-start(f32[2048]{0:T(1024)} %param.29) | copy-start | bytes 24580
  380.9 21.8 %copy-start.12 = (bf16[1408,256]{1,0:T(8,128)(2,1)S(1)}, bf16[1408,256]{1,0:T(8,128)(2,1)}, u32[]{:S(2)}) copy-start(bf16[1408,256]{1,0:T(8,128)(2,1)} %param.33) | copy-start | bytes 2162692
  380.9 48.2 %all-to-all-start.1 = ((bf16[8,256,704]{1,2,0:T(8,128)(2,1)}), bf16[8,256,704]{1,2,0:T(8,128)(2,1)}, u32[]{:S(2)}, u32[]{:S(2)}) async-start(bf16[8,256,704]{1,2,0:T(8,128)(2,1)} %copy.83), calls=%async_computation.2 | async-start | bytes 5767168 | tf_op jit(solution)/shard_map/all_to_all | solution.py:182
  386.6 57.5 %all-gather.6.cloned.1.call-start = ((), (), s32[]{:S(2)}) async-start(), calls=%async_computation.6 | async-start | bytes 2621440 | tf_op jit(solution)/shard_map/all_gather | solution.py:171
  415.0 31.1 %copy-start.20 = (f32[2,3,1408]{2,0,1:T(2,128)S(1)}, f32[2,3,1408]{2,0,1:T(2,128)}, u32[]{:S(2)}) copy-start(f32[2,3,1408]{2,0,1:T(2,128)} %param.32) | copy-start | bytes 101380
  429.1 59.4 %all-to-all-start.2 = ((bf16[704,8,256]{2,0,1:T(8,128)(2,1)}), bf16[704,8,256]{2,0,1:T(8,128)(2,1)}, u32[]{:S(2)}, u32[]{:S(2)}) async-start(bf16[704,8,256]{2,0,1:T(8,128)(2,1)} %copy.85), calls=%async_computation.3 | async-start | bytes 5767168 | tf_op jit(solution)/shard_map/all_to_all | solution.py:185
  444.0 202.8 %reduce-scatter.5.cloned.1.call-start = ((), (), s32[]{:S(2)}) async-start(), calls=%async_computation.7 | async-start | bytes 2621440 | tf_op jit(solution)/shard_map/reduce_scatter | solution.py:206
  444.1 55.9 %collective-permute-start = (bf16[512,2048]{1,0:T(8,128)(2,1)}, bf16[512,2048]{1,0:T(8,128)(2,1)}, u32[]{:S(2)}, u32[]{:S(2)}) collective-permute-start(bf16[512,2048]{1,0:T(8,128)(2,1)} %all-gather.6.cloned.1.call-done), channel_id=1, source_target_pairs={{0,4},{4,0},{8,12},{12,8},{16,20},{20,16},{24,28},{28,24},{1,5},{5... | collective-permute-start | bytes 6291464 | tf_op jit(solution)/shard_map/ppermute | solution.py:30
  453.8 46.2 %copy-start.11 = (bf16[512,2048]{1,0:T(8,128)(2,1)S(1)}, bf16[512,2048]{1,0:T(8,128)(2,1)}, u32[]{:S(2)}) copy-start(bf16[512,2048]{1,0:T(8,128)(2,1)} %all-gather.6.cloned.1.call-done) | copy-start | bytes 6291460
  490.7 11.2 %copy-start.10 = (bf16[8,88,8,256]{3,2,0,1:T(8,128)(2,1)S(1)}, bf16[8,88,8,256]{3,2,0,1:T(8,128)(2,1)}, u32[]{:S(2)}) copy-start(bf16[8,88,8,256]{3,2,0,1:T(8,128)(2,1)} %copy.99) | copy-start | bytes 8650756
  505.2 9.4 %collective-permute-start.1 = (bf16[2,704]{0,1:T(8,128)(2,1)S(1)}, bf16[2,704]{0,1:T(8,128)(2,1)S(1)}, u32[]{:S(2)}, u32[]{:S(2)}) collective-permute-start(bf16[2,704]{0,1:T(8,128)(2,1)S(1)} %slice.118), channel_id=1, source_target_pairs={{0,8},{4,12},{8,16},{12,20},{16,24},{20,28},{1,9},{5,13},{9,17},{1... | collective-permute-start | bytes 8456 | tf_op jit(solution)/shard_map/ppermute | solution.py:36
  511.2 6.4 collective-permute-start.2
  529.7 77.5 %collective-permute-start.3 = (f32[512,2048]{1,0:T(8,128)}, f32[512,2048]{1,0:T(8,128)}, u32[]{:S(2)}, u32[]{:S(2)}) collective-permute-start(f32[512,2048]{1,0:T(8,128)} %constant_dynamic-slice_fusion.4), channel_id=1, source_target_pairs={{0,4},{4,0},{8,12},{12,8},{16,20},{20,16},{24,28},{28,24},{1,5},{5... | collective-permute-start | bytes 12582920 | tf_op jit(solution)/shard_map/ppermute | solution.py:30
  530.3 116.6 %copy-start.6 = (bf16[128,2048]{1,0:T(8,128)(2,1)S(1)}, bf16[128,2048]{1,0:T(8,128)(2,1)}, u32[]{:S(2)}) copy-start(bf16[128,2048]{1,0:T(8,128)(2,1)} %reduce-scatter.3.cloned.1.call-done) | copy-start | bytes 1572868
  607.2 41.7 %copy-start.1 = (bf16[512,2048]{1,0:T(8,128)(2,1)S(1)}, bf16[512,2048]{1,0:T(8,128)(2,1)}, u32[]{:S(2)}) copy-start(bf16[512,2048]{1,0:T(8,128)(2,1)} %param.28) | copy-start | bytes 6291460
  (5 other events, 31.2 us)
Sparse Core Ops, SparseCore 0:
  367.1 32.1 reduce-scatter.2
  402.8 22.5 all-gather.5
  612.9 33.9 reduce-scatter.4
where the time goes:
time: 661 us; the launch traced here: 656 us
  waiting for transfers between devices  184 us (28%)
  matrix products  133 us (20%)
  blocking collectives  131 us (20%)
  local copies, waits for them, and re-layouts  111 us (17%)
  other arithmetic  45.4 us (7%)
  starting transfers between devices  36.8 us (6%)
  between operations  14.1 us (2%)
    all_gather x4, blocking collectives, entering(): pieces = jax.tree.map(lambda part: lax.all_gather(part, axis), value)  131 us
    ppermute x2, waiting for transfers between devices, from_partner(): return lax.ppermute(block, axis, route)  86.2 us
    dot_general x1, matrix products, state_mixer(): jnp.einsum('bkgp,ghp->bkgh', state_im, out_map[1], precision=highest)  35.4 us
    dot_general x1, matrix products, state_mixer(): jnp.einsum('bkgp,ghp->bkgh', state_re, out_map[0], precision=highest)  35.1 us
    all_to_all x1, waiting for transfers between devices, per_device(): lax.all_to_all(jnp.tile(paired_down, (1, copies)), 'sp', split_axis=1, co...  34.6 us
    reduce_scatter x1, waiting for transfers between devices, per_device(): lax.psum_scatter(block_total.astype(jnp.bfloat16), 'tp', scatter_dimensio...  34.1 us
    dynamic_slice x32, local copies, waits for them, and re-layouts, state_mixer(): final, starts = lax.scan(advance, (zeros, zeros, ones, zeros), items)  31.9 us
    dot_general x1, matrix products, state_mixer(): jnp.einsum('kl,blgp->bkgp', lower_ones, scaled_im, precision=highest)  20.1 us
  transfers between devices with their start and end apart: 10, of which 7 were waited for; matrix products, arithmetic and copies ran while one was open for 36% of the time, Pallas kernels for 0%

commit v1 on v0

v1 whole, which is shorter than its diff:
```python
import functools

import jax
import jax.numpy as jnp
from jax import lax
from jax.experimental import pallas as pl
from jax.experimental.pallas import tpu as pltpu
from jax.sharding import PartitionSpec as P

CONV = 3
SUB = 8
LANE_BLOCK = 512
MESH = pl.DeviceIdType.MESH


def complex_power(re, im, exponent):
    out = None
    while exponent:
        if exponent & 1:
            out = (
                (re, im)
                if out is None
                else (out[0] * re - out[1] * im, out[0] * im + out[1] * re)
            )
        exponent >>= 1
        if exponent:
            re, im = (re * re - im * im, 2.0 * re * im)
    return out


def mixer_kernel(
    ring,
    states,
    x_ref,
    damp_ref,
    abar_re_ref,
    abar_im_ref,
    in_re_ref,
    in_im_ref,
    out_re_ref,
    out_im_ref,
    skip_ref,
    w_out_ref,
    proj_ref,
    growth,
    state_re,
    state_im,
    begin_re,
    begin_im,
    outbox,
    inbox,
    send_sem,
    recv_sem,
):
    bf16, f32 = (jnp.bfloat16, jnp.float32)
    me = lax.axis_index("sp")
    barrier = pltpu.get_barrier_semaphore()
    for apart in range(1, ring):
        peer = lax.rem(me + apart, ring)
        pl.semaphore_signal(barrier, inc=1, device_id={"sp": peer}, device_id_type=MESH)
    tokens = x_ref.shape[0]
    lanes = growth.shape[1]
    steps = tokens // SUB
    rows = lax.broadcasted_iota(jnp.int32, (tokens, tokens), 0)
    cols = lax.broadcasted_iota(jnp.int32, (tokens, tokens), 1)
    spread = (cols == (rows % SUB) * steps + rows // SUB).astype(bf16)
    gather = (rows == (cols % SUB) * steps + cols // SUB).astype(bf16)
    x_perm = jnp.dot(spread, x_ref[...], preferred_element_type=f32).astype(bf16)
    factor = jnp.exp(damp_ref[...])
    high = factor.astype(bf16)
    rest = factor - high.astype(f32)
    middle = rest.astype(bf16)
    low = (rest - middle.astype(f32)).astype(bf16)
    groups = factor.shape[1]
    pick = (
        lax.broadcasted_iota(jnp.int32, (groups, lanes), 1) // states
        == lax.broadcasted_iota(jnp.int32, (groups, lanes), 0)
    ).astype(bf16)
    total = None
    for part in (high, middle, low):
        moved = jnp.dot(spread, part, preferred_element_type=f32).astype(bf16)
        wide = jnp.dot(moved, pick, preferred_element_type=f32)
        total = wide if total is None else total + wide
    growth[...] = total
    blocks = in_re_ref.shape[0]
    width = in_re_ref.shape[1]
    span = in_re_ref.shape[2]
    for b in range(blocks):
        piece = x_perm[:, b * width : (b + 1) * width]
        state_re[:, b * span : (b + 1) * span] = jnp.dot(
            piece, in_re_ref[b], preferred_element_type=f32
        )
        state_im[:, b * span : (b + 1) * span] = jnp.dot(
            piece, in_im_ref[b], preferred_element_type=f32
        )

    def advance(start, keep, cut, re, im, a_re, a_im):
        row = pl.multiple_of(start * SUB, SUB)
        grow = growth[pl.ds(row, SUB), cut]
        re, im = (re * grow, im * grow)
        new_re = a_re * re - a_im * im + state_re[pl.ds(row, SUB), cut]
        new_im = a_re * im + a_im * re + state_im[pl.ds(row, SUB), cut]
        if keep:
            state_re[pl.ds(row, SUB), cut] = new_re
            state_im[pl.ds(row, SUB), cut] = new_im
        return (new_re, new_im, grow)

    total_re, total_im = complex_power(abar_re_ref[...], abar_im_ref[...], steps)
    local = []
    for lane in range(0, lanes, LANE_BLOCK):
        cut = slice(lane, lane + LANE_BLOCK)
        a_re = jnp.broadcast_to(abar_re_ref[:, cut], (SUB, LANE_BLOCK))
        a_im = jnp.broadcast_to(abar_im_ref[:, cut], (SUB, LANE_BLOCK))

        def body(step, carry):
            re, im, grown = carry
            re, im, grow = advance(step, False, cut, re, im, a_re, a_im)
            return (re, im, grown * grow)

        zero = jnp.zeros((SUB, LANE_BLOCK), f32)
        re, im, grown = lax.fori_loop(
            0, steps, body, (zero, zero, jnp.ones((SUB, LANE_BLOCK), f32)), unroll=4
        )
        local.append((re, im, grown * total_re[:, cut], grown * total_im[:, cut]))
    fin_re, fin_im, jump_re, jump_im = [
        jnp.concatenate([item[k] for item in local], axis=1) for k in range(4)
    ]
    at_re, at_im = (fin_re[0:1], fin_im[0:1])
    all_re, all_im = (jump_re[0:1], jump_im[0:1])
    for c in range(1, SUB):
        j_re, j_im = (jump_re[c : c + 1], jump_im[c : c + 1])
        at_re, at_im = (
            j_re * at_re - j_im * at_im + fin_re[c : c + 1],
            j_re * at_im + j_im * at_re + fin_im[c : c + 1],
        )
        all_re, all_im = (j_re * all_re - j_im * all_im, j_re * all_im + j_im * all_re)
    outbox[0:1, :] = at_re
    outbox[1:2, :] = at_im
    outbox[2:3, :] = all_re
    outbox[3:4, :] = all_im
    pl.semaphore_wait(barrier, ring - 1)
    copies = []
    for apart in range(1, ring):
        copy = pltpu.make_async_remote_copy(
            src_ref=outbox,
            dst_ref=inbox.at[apart],
            send_sem=send_sem.at[apart],
            recv_sem=recv_sem.at[apart],
            device_id={"sp": lax.rem(me + apart, ring)},
            device_id_type=MESH,
        )
        copy.start()
        copies.append(copy)
    for copy in copies:
        copy.wait()
    at_re = jnp.zeros((1, lanes), f32)
    at_im = jnp.zeros((1, lanes), f32)
    for apart in range(ring - 1, 0, -1):
        f_re, f_im = (inbox[apart, 0:1, :], inbox[apart, 1:2, :])
        j_re, j_im = (inbox[apart, 2:3, :], inbox[apart, 3:4, :])
        valid = me >= apart
        new_re = j_re * at_re - j_im * at_im + f_re
        new_im = j_re * at_im + j_im * at_re + f_im
        at_re = jnp.where(valid, new_re, at_re)
        at_im = jnp.where(valid, new_im, at_im)
    for c in range(SUB):
        begin_re[c : c + 1, :] = at_re
        begin_im[c : c + 1, :] = at_im
        if c < SUB - 1:
            j_re, j_im = (jump_re[c : c + 1], jump_im[c : c + 1])
            at_re, at_im = (
                j_re * at_re - j_im * at_im + fin_re[c : c + 1],
                j_re * at_im + j_im * at_re + fin_im[c : c + 1],
            )
    for lane in range(0, lanes, LANE_BLOCK):
        cut = slice(lane, lane + LANE_BLOCK)
        a_re = jnp.broadcast_to(abar_re_ref[:, cut], (SUB, LANE_BLOCK))
        a_im = jnp.broadcast_to(abar_im_ref[:, cut], (SUB, LANE_BLOCK))

        def body(step, carry):
            re, im, _ = advance(step, True, cut, *carry, a_re, a_im)
            return (re, im)

        lax.fori_loop(0, steps, body, (begin_re[:, cut], begin_im[:, cut]), unroll=4)
    pieces = []
    for b in range(blocks):
        cut = slice(b * span, (b + 1) * span)
        here = slice(b * width, (b + 1) * width)
        mixed = (
            jnp.dot(state_re[:, cut].astype(bf16), out_re_ref[b], preferred_element_type=f32)
            - jnp.dot(state_im[:, cut].astype(bf16), out_im_ref[b], preferred_element_type=f32)
            + skip_ref[:, here] * x_perm[:, here].astype(f32)
        )
        pieces.append(jax.nn.gelu(mixed).astype(bf16))
    activated = jnp.dot(
        gather, jnp.concatenate(pieces, axis=1), preferred_element_type=f32
    ).astype(bf16)
    columns = w_out_ref.shape[1]
    piece = min(512, columns)

    def project(k, _):
        there = pl.ds(pl.multiple_of(k * piece, piece), piece)
        proj_ref[:, there] = jnp.dot(
            activated, w_out_ref[:, there], preferred_element_type=f32
        ).astype(bf16)
        return 0

    lax.fori_loop(0, columns // piece, project, 0)


def block_diagonal(parts, per_block):
    groups, rows, cols = parts.shape
    blocks = groups // per_block
    eye = jnp.eye(per_block, dtype=parts.dtype)
    wide = (
        parts.reshape(blocks, per_block, rows, 1, cols) * eye[None, :, None, :, None]
    )
    return wide.reshape(blocks, per_block * rows, per_block * cols).astype(jnp.bfloat16)


def state_projection(
    mixer_input, log_step, rate_real, rate_imag, damping, in_map, out_map, skip, w_out
):
    tokens_here, channels = mixer_input.shape
    groups_here, states = rate_real.shape
    group_width = channels // groups_here
    step_size = jnp.exp(log_step)[:, None]
    log_rate = rate_real * step_size
    angle_step = rate_imag * step_size
    magnitude = jnp.exp(log_rate)
    abar_re = magnitude * jnp.cos(angle_step)
    abar_im = magnitude * jnp.sin(angle_step)
    denominator = rate_real * rate_real + rate_imag * rate_imag
    minus_one = abar_re - 1.0
    factor_re = (minus_one * rate_real + abar_im * rate_imag) / denominator
    factor_im = (abar_im * rate_real - minus_one * rate_imag) / denominator
    bbar_re = factor_re[..., None] * in_map[0] - factor_im[..., None] * in_map[1]
    bbar_im = factor_re[..., None] * in_map[1] + factor_im[..., None] * in_map[0]
    per_block = 128 // group_width
    lanes = groups_here * states
    ring = lax.axis_size("sp")
    vmem = pl.BlockSpec(memory_space=pltpu.VMEM)
    f32 = jnp.float32
    return pl.pallas_call(
        functools.partial(mixer_kernel, ring, states),
        out_shape=jax.ShapeDtypeStruct((tokens_here, w_out.shape[1]), jnp.bfloat16),
        in_specs=[vmem] * 10,
        out_specs=vmem,
        scratch_shapes=[
            pltpu.VMEM((tokens_here, lanes), f32),
            pltpu.VMEM((tokens_here, lanes), f32),
            pltpu.VMEM((tokens_here, lanes), f32),
            pltpu.VMEM((SUB, lanes), f32),
            pltpu.VMEM((SUB, lanes), f32),
            pltpu.VMEM((4, lanes), f32),
            pltpu.VMEM((ring, 4, lanes), f32),
            pltpu.SemaphoreType.DMA((ring,)),
            pltpu.SemaphoreType.DMA((ring,)),
        ],
        compiler_params=pltpu.CompilerParams(
            collective_id=0, has_side_effects=True, vmem_limit_bytes=56 * 1024 * 1024
        ),
        cost_estimate=pl.CostEstimate(
            flops=20_000_000_000, bytes_accessed=8_000_000, transcendentals=0
        ),
        name="state_projection",
    )(
        mixer_input,
        damping,
        abar_re.reshape(1, lanes),
        abar_im.reshape(1, lanes),
        block_diagonal(jnp.swapaxes(bbar_re, 1, 2), per_block),
        block_diagonal(jnp.swapaxes(bbar_im, 1, 2), per_block),
        block_diagonal(jnp.swapaxes(out_map[0], 1, 2), per_block),
        block_diagonal(jnp.swapaxes(out_map[1], 1, 2), per_block),
        skip.reshape(1, channels),
        w_out,
    )


def from_partner(block, axis, apart):
    count = lax.axis_size(axis)
    route = []
    for low in range(count):
        high = low | 1 << apart
        if high != low and high < count:
            route += [(low, high), (high, low)]
    return lax.ppermute(block, axis, route)


def from_behind(value, axis, steps):
    count = lax.axis_size(axis)
    initial, last = (max(0, -steps), min(count, count - steps))
    return lax.ppermute(value, axis, [(source, source + steps) for source in range(initial, last)])


def normalize(stream, norm_gain):
    stream_f = stream.astype(jnp.float32)
    scale = lax.rsqrt(jnp.mean(stream_f * stream_f, axis=-1, keepdims=True) + 1e-06)
    return (stream_f * scale * norm_gain).astype(jnp.bfloat16)


def causal_conv(act_pre, lin_pre, previous, taps):
    row_count, width = act_pre.shape
    act_pad = jnp.concatenate([previous[0], act_pre], axis=0).astype(jnp.float32)
    lin_pad = jnp.concatenate([previous[1], lin_pre], axis=0).astype(jnp.float32)
    act_conv = jnp.zeros((row_count, width), jnp.float32)
    lin_conv = jnp.zeros((row_count, width), jnp.float32)
    for offset in range(CONV):
        act_conv = act_conv + taps[0, offset][None, :] * act_pad[offset : offset + row_count]
        lin_conv = lin_conv + taps[1, offset][None, :] * lin_pad[offset : offset + row_count]
    return (jax.nn.silu(act_conv) * lin_conv).astype(jnp.bfloat16)


def per_device(
    mixer_input,
    residual,
    log_step,
    rate_real,
    rate_imag,
    damping,
    in_map,
    out_map,
    skip,
    w_out,
    norm_gain,
    w_act,
    w_lin,
    conv_taps,
    w_down,
):
    tokens_here = mixer_input.shape[0]
    hidden_here = w_act.shape[1]
    partial_projection = state_projection(
        mixer_input, log_step, rate_real, rate_imag, damping, in_map, out_map, skip, w_out
    )
    projected = lax.psum_scatter(
        partial_projection,
        "tp",
        scatter_dimension=0,
        tiled=True,
    ).astype(jnp.float32)
    stream = (residual.astype(jnp.float32) + projected).astype(jnp.bfloat16)
    normed_all = lax.all_gather(normalize(stream, norm_gain), "tp", axis=0, tiled=True)
    parity = lax.axis_index("sp") % 2
    half = hidden_here // 2
    copies = lax.axis_size("sp") // 2

    def outgoing_rows(weight):
        paired = jnp.concatenate([weight[:, :half], weight[:, half:]], axis=0)
        return jnp.tile(paired, (copies, 1))

    act_half, lin_half = (
        lax.all_to_all(outgoing_rows(w_act), "sp", split_axis=0, concat_axis=0, tiled=True),
        lax.all_to_all(outgoing_rows(w_lin), "sp", split_axis=0, concat_axis=0, tiled=True),
    )
    paired_down = jnp.concatenate([w_down[:half], w_down[half:]], axis=1)
    down_half = lax.all_to_all(
        jnp.tile(paired_down, (1, copies)), "sp", split_axis=1, concat_axis=1, tiled=True
    )
    partner = from_partner(normed_all, "sp", 0)
    first = jnp.where(parity == 0, normed_all, partner)
    second = jnp.where(parity == 0, partner, normed_all)
    normed_pair = jnp.concatenate([first, second], axis=0)
    act_pre = jnp.dot(normed_pair, act_half, preferred_element_type=jnp.float32).astype(
        jnp.bfloat16
    )
    lin_pre = jnp.dot(normed_pair, lin_half, preferred_element_type=jnp.float32).astype(
        jnp.bfloat16
    )
    edge = 2 * tokens_here - (CONV - 1)
    previous = from_behind((act_pre[edge:], lin_pre[edge:]), "sp", 2)
    taps = lax.dynamic_slice_in_dim(conv_taps, parity * half, half, 2)
    hidden = causal_conv(act_pre, lin_pre, previous, taps)
    partial_value = jnp.dot(hidden, down_half, preferred_element_type=jnp.float32)
    mine = lax.dynamic_slice_in_dim(partial_value, parity * tokens_here, tokens_here, 0)
    other = lax.dynamic_slice_in_dim(partial_value, (1 - parity) * tokens_here, tokens_here, 0)
    block_total = mine + from_partner(other, "sp", 0)
    channel_sum = lax.psum_scatter(
        block_total.astype(jnp.bfloat16), "tp", scatter_dimension=0, tiled=True
    ).astype(jnp.float32)
    return (stream.astype(jnp.float32) + channel_sum).astype(jnp.bfloat16)


def solution(mesh):
    in_specs = (
        P("sp", "tp"),
        P(("sp", "tp"), None),
        P("tp"),
        P("tp", None),
        P("tp", None),
        P("sp", "tp"),
        P(None, "tp", None, None),
        P(None, "tp", None, None),
        P("tp"),
        P("tp", None),
        P(),
        P("sp", "tp"),
        P("sp", "tp"),
        P(None, None, "tp"),
        P("tp", "sp"),
    )
    out_specs = P(("sp", "tp"), None)
    return jax.shard_map(
        per_device, mesh=mesh, in_specs=in_specs, out_specs=out_specs, check_vma=False
    )
```

time: 661 us -> 442 us (0.67)
  blocking collectives: 131 us -> 0 us
  matrix products: 133 us -> 13.2 us
  waiting for transfers between devices: 184 us -> 241 us
  Pallas kernels: 0 us -> 42.8 us
  local copies, waits for them, and re-layouts: 111 us -> 83.1 us
  other arithmetic: 45.4 us -> 21.2 us
  starting transfers between devices: 36.8 us -> 25.7 us
    all_gather x4 -> x0, blocking collectives: 131 us -> none  [entering(): pieces = jax.tree.map(lambda part: lax.all_gather(part, axis), value)]
    dot_general x7 -> x0, matrix products: 120 us -> none  [the longest x1 35.4 us: state_mixer(): jnp.einsum('bkgp,ghp->bkgh', state_im, out_map[1], precision=highest)]
    pallas_call x0 -> x1, Pallas kernels: none -> 42.8 us  [state_projection(): pl.pallas_call(functools.partial(mixer_kernel, ring, states), out_shape=j...]
    dynamic_slice x32 -> x0, local copies, waits for them, and re-layouts: 31.9 us -> none  [state_mixer(): final, starts = lax.scan(advance, (zeros, zeros, ones, zeros), items)]
    mul x1 -> x17, local copies, waits for them, and re-layouts: 0.08 us -> 25.7 us  [block_diagonal(): parts.reshape(blocks, per_block, rows, 1, cols)]
    all_to_all x1, waiting for transfers between devices: 14.1 us -> 39.7 us  [per_device(): lax.all_to_all(outgoing_rows(w_lin), 'sp', split_axis=0, concat_axis=0, t...]
    all_to_all x1, waiting for transfers between devices: 34.6 us -> 56.7 us  [per_device(): lax.all_to_all(jnp.tile(paired_down, (1, copies)), 'sp', split_axis=1, co...]
    dynamic_update_slice x32 -> x0, other arithmetic: 19.7 us -> none  [state_mixer(): final, starts = lax.scan(advance, (zeros, zeros, ones, zeros), items)]
  transfers between devices with their start and end apart: 10 -> 10, of which waited for: 7 -> 7; matrix products, arithmetic and copies ran while one was open for 36% -> 16% of each run, Pallas kernels for 0% -> 10%
where the time goes in v1:
time: 442 us; the launch traced here: 441 us
  waiting for transfers between devices  241 us (55%)
  local copies, waits for them, and re-layouts  83.1 us (19%)
  Pallas kernels  42.8 us (10%)
  starting transfers between devices  25.7 us (6%)
  other arithmetic  21.2 us (5%)
  between operations  13.4 us (3%)
  matrix products  13.2 us (3%)
    ppermute x2, waiting for transfers between devices, from_partner(): return lax.ppermute(block, axis, route)  102 us
    all_to_all x1, waiting for transfers between devices, per_device(): lax.all_to_all(jnp.tile(paired_down, (1, copies)), 'sp', split_axis=1, co...  56.7 us
    pallas_call x1, Pallas kernels, state_projection(): pl.pallas_call(functools.partial(mixer_kernel, ring, states), out_shape=j...  42.8 us
    all_to_all x1, waiting for transfers between devices, per_device(): lax.all_to_all(outgoing_rows(w_lin), 'sp', split_axis=0, concat_axis=0, t...  39.7 us
    reduce_scatter x1, waiting for transfers between devices, per_device(): lax.psum_scatter(block_total.astype(jnp.bfloat16), 'tp', scatter_dimensio...  31.1 us
    mul x17, local copies, waits for them, and re-layouts, block_diagonal(): parts.reshape(blocks, per_block, rows, 1, cols)  25.7 us
    all_to_all x3, local copies, waits for them, and re-layouts, per_device(): lax.all_to_all(outgoing_rows(w_lin), 'sp', split_axis=0, concat_axis=0, t...  13.6 us
    all_to_all x3, local copies, waits for them, and re-layouts, per_device(): lax.all_to_all(jnp.tile(paired_down, (1, copies)), 'sp', split_axis=1, co...  12.3 us
  transfers between devices with their start and end apart: 10, of which 7 were waited for; matrix products, arithmetic and copies ran while one was open for 16% of the time, Pallas kernels for 10%

profile of v1, /device:TPU:0, one launch (start us, length us, event | category | flops | bytes accessed | tf_op | source)
XLA Modules:
  0.0 440.6 jit_solution(9175793580674156830)
XLA Ops:
  13.3 4.0 copy.41
  17.3 7.4 %all-to-all-start = ((bf16[8,256,704]{1,2,0:T(8,128)(2,1)}), bf16[8,256,704]{1,2,0:T(8,128)(2,1)S(1)}, u32[]{:S(2)}, u32[]{:S(2)}) async-start(bf16[8,256,704]{1,2,0:T(8,128)(2,1)} %copy.41), calls=%async_computation.1 | async-start | bytes 5767168 | tf_op jit(solution)/shard_map/all_to_all | solution.py:354
  27.6 2.7 mul.266
  32.0 2.7 mul.275
  38.5 2.8 mul.279
  41.3 2.6 copy.36
  45.5 2.8 mul.286
  48.3 2.5 copy.38
  55.1 3.1 multiply_convert_fusion.2
  59.4 42.8 %state_projection.1 = bf16[512,2048]{1,0:T(8,128)(2,1)} custom-call(bf16[512,512]{1,0:T(8,128)(2,1)} %x_ref.1, f32[512,32]{1,0:T(8,128)} %copy.39.damp_ref, f32[1,2048]{1,0:T(1,128)} %reshape.76.abar_re_ref, f32[1,2048]{1,0:T(1,128)} %reshape.77.abar_im_ref, bf16[4,128,512]{2,1,0:T(8,128)(2,1)} %get-tuple-element.26.in_re_ref, ...), custom_call_target="tpu_custom_call" | custom-call | flops 20000000000 | bytes 8000000 | tf_op jit(solution)/shard_map/state_projection/pallas_call | solution.py:244
  106.7 3.5 tile.7
  110.2 5.8 %all_to_all.27 = bf16[8,256,704]{1,0,2:T(8,128)(2,1)} reshape(bf16[4,512,704]{1,0,2:T(4,128)(2,1)} %tile.7) | data formatting | bytes 5767168 | tf_op jit(solution)/shard_map/all_to_all | solution.py:355
  116.0 4.0 copy.44
  120.0 4.8 %all-to-all-start.1 = ((bf16[8,256,704]{1,2,0:T(8,128)(2,1)}), bf16[8,256,704]{1,2,0:T(8,128)(2,1)}, u32[]{:S(2)}, u32[]{:S(2)}) async-start(bf16[8,256,704]{1,2,0:T(8,128)(2,1)} %copy.44), calls=%async_computation.2 | async-start | bytes 5767168 | tf_op jit(solution)/shard_map/all_to_all | solution.py:355
  124.9 8.7 %reduce-scatter.3.cloned.1.call-done = bf16[128,2048]{1,0:T(8,128)(2,1)} async-done(((bf16[512,2048]{1,0:T(8,128)(2,1)}), bf16[128,2048]{1,0:T(8,128)(2,1)}) %reduce-scatter.3.cloned.1.call-update) | async-done | bytes 524304 | tf_op jit(solution)/shard_map/reduce_scatter | solution.py:337
  140.5 5.9 %all_to_all.30 = bf16[704,8,256]{2,1,0:T(8,128)(2,1)} reshape(bf16[704,4,512]{2,1,0:T(4,128)(2,1)} %tile.8) | data formatting | bytes 5767168 | tf_op jit(solution)/shard_map/all_to_all | solution.py:358
  146.5 4.0 copy.46
  150.5 39.7 %all-to-all-done.1 = bf16[8,256,704]{1,2,0:T(8,128)(2,1)} async-done(((bf16[8,256,704]{1,2,0:T(8,128)(2,1)}), bf16[8,256,704]{1,2,0:T(8,128)(2,1)}, u32[]{:S(2)}, u32[]{:S(2)}) %all-to-all-start.1) | async-done | bytes 2883616 | tf_op jit(solution)/shard_map/all_to_all | solution.py:355
  190.2 4.4 %all-to-all-start.2 = ((bf16[704,8,256]{2,0,1:T(8,128)(2,1)}), bf16[704,8,256]{2,0,1:T(8,128)(2,1)}, u32[]{:S(2)}, u32[]{:S(2)}) async-start(bf16[704,8,256]{2,0,1:T(8,128)(2,1)} %copy.46), calls=%async_computation.3 | async-start | bytes 5767168 | tf_op jit(solution)/shard_map/all_to_all | solution.py:358
  198.7 3.8 copy.49
  202.6 56.7 %all-to-all-done.2 = bf16[704,8,256]{2,0,1:T(8,128)(2,1)} async-done(((bf16[704,8,256]{2,0,1:T(8,128)(2,1)}), bf16[704,8,256]{2,0,1:T(8,128)(2,1)}, u32[]{:S(2)}, u32[]{:S(2)}) %all-to-all-start.2) | async-done | bytes 2883616 | tf_op jit(solution)/shard_map/all_to_all | solution.py:358
  261.7 10.7 %collective-permute-done = bf16[512,2048]{1,0:T(8,128)(2,1)} collective-permute-done((bf16[512,2048]{1,0:T(8,128)(2,1)}, bf16[512,2048]{1,0:T(8,128)(2,1)}, u32[]{:S(2)}, u32[]{:S(2)}) %collective-permute-start) | collective-permute-done | bytes 2097184 | tf_op jit(solution)/shard_map/ppermute | solution.py:288
  274.5 3.2 fusion.8
  277.8 3.4 collective-permute-start.1
  281.2 3.2 fusion.9
  284.5 3.6 collective-permute-start.2
  289.0 2.6 collective-permute-done.2
  292.4 6.8 %fusion.10 = f32[1024,2048]{1,0:T(8,128)S(1)} fusion(bf16[704,2048]{1,0:T(8,128)(2,1)S(1)} %bitcast.63, f32[1026,704]{0,1:T(8,128)S(1)} %maximum_convert_fusion.1, f32[1026,704]{0,1:T(8,128)S(1)} %maximum_convert_fusion, f32[704]{0:T(1024)S(1)} %get-tuple-element.10, f32[704]{0:T(1024)S(1)} %get-tuple-element.6, f32[704]{0:T(1024)S(1)} %get-tuple-element.7, ...), kind=kOutput, calls=%fused_computation.25 | convolution fusion | flops 2964324352 | bytes 28598272 | tf_op jit(solution)/shard_map/dot_general | solution.py:375
  299.2 2.4 constant_dynamic-slice_fusion
  303.7 91.7 %collective-permute-done.3 = f32[512,2048]{1,0:T(8,128)} collective-permute-done((f32[512,2048]{1,0:T(8,128)}, f32[512,2048]{1,0:T(8,128)}, u32[]{:S(2)}, u32[]{:S(2)}) %collective-permute-start.3) | collective-permute-done | bytes 4194336 | tf_op jit(solution)/shard_map/ppermute | solution.py:288
  395.4 5.4 %add_convert_fusion = bf16[512,2048]{1,0:T(8,128)(2,1)} fusion(f32[512,2048]{1,0:T(8,128)} %collective-permute-done.3, f32[1024,2048]{1,0:T(8,128)} %copy-done, s32[]{:T(128)S(6)} %select_n.33), kind=kLoop, calls=%fused_computation.1 | loop fusion | flops 2097152 | bytes 10485764 | tf_op jit(solution)/shard_map/convert_element_type | solution.py:380
  400.8 31.1 %reduce-scatter.5.cloned.1.call-done = bf16[128,2048]{1,0:T(8,128)(2,1)} async-done(((bf16[512,2048]{1,0:T(8,128)(2,1)}), bf16[128,2048]{1,0:T(8,128)(2,1)}) %reduce-scatter.5.cloned.1.call-update) | async-done | bytes 524304 | tf_op jit(solution)/shard_map/reduce_scatter | solution.py:379
  (83 shorter events, 48.2 us)
Async XLA Ops:
  17.3 7.5 %copy-start.13 = (f32[32]{0:T(128)S(1)}, f32[32]{0:T(128)}, u32[]{:S(2)}) copy-start(f32[32]{0:T(128)} %param.17) | copy-start | bytes 388
  17.3 7.5 %copy-start.9 = (f32[32,64]{1,0:T(8,128)S(1)}, f32[32,64]{1,0:T(8,128)}, u32[]{:S(2)}) copy-start(f32[32,64]{1,0:T(8,128)} %param.19) | copy-start | bytes 24580
  17.3 7.5 %copy-start.10 = (f32[32,64]{1,0:T(8,128)S(1)}, f32[32,64]{1,0:T(8,128)}, u32[]{:S(2)}) copy-start(f32[32,64]{1,0:T(8,128)} %param.18) | copy-start | bytes 24580
  17.3 102.8 %all-to-all-start = ((bf16[8,256,704]{1,2,0:T(8,128)(2,1)}), bf16[8,256,704]{1,2,0:T(8,128)(2,1)S(1)}, u32[]{:S(2)}, u32[]{:S(2)}) async-start(bf16[8,256,704]{1,2,0:T(8,128)(2,1)} %copy.41), calls=%async_computation.1 | async-start | bytes 5767168 | tf_op jit(solution)/shard_map/all_to_all | solution.py:354
  24.7 108.9 %reduce-scatter.3.cloned.1.call-start = ((), (), s32[]{:S(2)}) async-start(), calls=%async_computation.5 | async-start | bytes 2621440 | tf_op jit(solution)/shard_map/reduce_scatter | solution.py:337
  45.5 8.8 %copy-start.8 = (f32[512,32]{0,1:T(8,128)S(1)}, f32[512,32]{0,1:T(8,128)}, u32[]{:S(2)}) copy-start(f32[512,32]{0,1:T(8,128)} %param.20) | copy-start | bytes 196612
  55.1 3.1 copy-start.3
  55.1 3.1 copy-start.4
  120.0 13.6 %copy-start.1 = (bf16[128,2048]{1,0:T(8,128)(2,1)S(1)}, bf16[128,2048]{1,0:T(8,128)(2,1)}, u32[]{:S(2)}) copy-start(bf16[128,2048]{1,0:T(8,128)(2,1)} %param.16) | copy-start | bytes 1572868
  120.0 14.9 %copy-start.12 = (f32[2048]{0:T(1024)S(1)}, f32[2048]{0:T(1024)}, u32[]{:S(2)}) copy-start(f32[2048]{0:T(1024)} %param.25) | copy-start | bytes 24580
  120.0 70.2 %all-to-all-start.1 = ((bf16[8,256,704]{1,2,0:T(8,128)(2,1)}), bf16[8,256,704]{1,2,0:T(8,128)(2,1)}, u32[]{:S(2)}, u32[]{:S(2)}) async-start(bf16[8,256,704]{1,2,0:T(8,128)(2,1)} %copy.44), calls=%async_computation.2 | async-start | bytes 5767168 | tf_op jit(solution)/shard_map/all_to_all | solution.py:355
  124.9 69.8 %all-gather.2.cloned.1.call-start = ((), (), s32[]{:S(2)}) async-start(), calls=%async_computation.6 | async-start | bytes 2621440 | tf_op jit(solution)/shard_map/all_gather | solution.py:344
  150.5 46.1 %copy-start.11 = (f32[2,3,1408]{2,0,1:T(2,128)S(1)}, f32[2,3,1408]{2,0,1:T(2,128)}, u32[]{:S(2)}) copy-start(f32[2,3,1408]{2,0,1:T(2,128)} %param.28) | copy-start | bytes 101380
  190.2 69.1 %all-to-all-start.2 = ((bf16[704,8,256]{2,0,1:T(8,128)(2,1)}), bf16[704,8,256]{2,0,1:T(8,128)(2,1)}, u32[]{:S(2)}, u32[]{:S(2)}) async-start(bf16[704,8,256]{2,0,1:T(8,128)(2,1)} %copy.46), calls=%async_computation.3 | async-start | bytes 5767168 | tf_op jit(solution)/shard_map/all_to_all | solution.py:358
  194.6 237.3 %reduce-scatter.5.cloned.1.call-start = ((), (), s32[]{:S(2)}) async-start(), calls=%async_computation.7 | async-start | bytes 2621440 | tf_op jit(solution)/shard_map/reduce_scatter | solution.py:379
  194.7 77.6 %collective-permute-start = (bf16[512,2048]{1,0:T(8,128)(2,1)}, bf16[512,2048]{1,0:T(8,128)(2,1)}, u32[]{:S(2)}, u32[]{:S(2)}) collective-permute-start(bf16[512,2048]{1,0:T(8,128)(2,1)} %all-gather.2.cloned.1.call-done), channel_id=1, source_target_pairs={{0,4},{4,0},{8,12},{12,8},{16,20},{20,16},{24,28},{28,24},{1,5},{5... | collective-permute-start | bytes 6291464 | tf_op jit(solution)/shard_map/ppermute | solution.py:288
  259.3 13.0 %copy-start.7 = (bf16[512,2048]{1,0:T(8,128)(2,1)S(1)}, bf16[512,2048]{1,0:T(8,128)(2,1)}, u32[]{:S(2)}) copy-start(bf16[512,2048]{1,0:T(8,128)(2,1)} %all-gather.2.cloned.1.call-done) | copy-start | bytes 6291460
  261.6 12.8 %copy-start.6 = (bf16[8,88,8,256]{3,2,0,1:T(8,128)(2,1)S(1)}, bf16[8,88,8,256]{3,2,0,1:T(8,128)(2,1)}, u32[]{:S(2)}) copy-start(bf16[8,88,8,256]{3,2,0,1:T(8,128)(2,1)} %copy.48) | copy-start | bytes 8650756
  274.5 6.7 %copy-start.5 = (bf16[8,88,8,256]{3,2,0,1:T(8,128)(2,1)S(1)}, bf16[8,88,8,256]{3,2,0,1:T(8,128)(2,1)}, u32[]{:S(2)}) copy-start(bf16[8,88,8,256]{3,2,0,1:T(8,128)(2,1)} %copy.49) | copy-start | bytes 8650756
  277.8 10.4 %collective-permute-start.1 = (bf16[2,704]{0,1:T(8,128)(2,1)S(1)}, bf16[2,704]{0,1:T(8,128)(2,1)S(1)}, u32[]{:S(2)}, u32[]{:S(2)}) collective-permute-start(bf16[2,704]{0,1:T(8,128)(2,1)S(1)} %slice.98), channel_id=1, source_target_pairs={{0,8},{4,12},{8,16},{12,20},{16,24},{20,28},{1,9},{5,13},{9,17},{1... | collective-permute-start | bytes 8456 | tf_op jit(solution)/shard_map/ppermute | solution.py:294
  284.5 7.1 %collective-permute-start.2 = (bf16[2,704]{0,1:T(8,128)(2,1)S(1)}, bf16[2,704]{0,1:T(8,128)(2,1)S(1)}, u32[]{:S(2)}, u32[]{:S(2)}) collective-permute-start(bf16[2,704]{0,1:T(8,128)(2,1)S(1)} %slice.102), channel_id=1, source_target_pairs={{0,8},{4,12},{8,16},{12,20},{16,24},{20,28},{1,9},{5,13},{9,17},{1... | collective-permute-start | bytes 8456 | tf_op jit(solution)/shard_map/ppermute | solution.py:294
  299.2 4.5 %copy-start = (f32[1024,2048]{1,0:T(8,128)}, f32[1024,2048]{1,0:T(8,128)S(1)}, u32[]{:S(2)}) copy-start(f32[1024,2048]{1,0:T(8,128)S(1)} %fusion.10) | copy-start | bytes 25165828
  303.7 91.7 %collective-permute-start.3 = (f32[512,2048]{1,0:T(8,128)}, f32[512,2048]{1,0:T(8,128)}, u32[]{:S(2)}, u32[]{:S(2)}) collective-permute-start(f32[512,2048]{1,0:T(8,128)} %constant_dynamic-slice_fusion), channel_id=1, source_target_pairs={{0,4},{4,0},{8,12},{12,8},{16,20},{20,16},{24,28},{28,24},{1,5},{5... | collective-permute-start | bytes 12582920 | tf_op jit(solution)/shard_map/ppermute | solution.py:288
  303.7 128.3 %copy-start.2 = (bf16[128,2048]{1,0:T(8,128)(2,1)S(1)}, bf16[128,2048]{1,0:T(8,128)(2,1)}, u32[]{:S(2)}) copy-start(bf16[128,2048]{1,0:T(8,128)(2,1)} %reduce-scatter.3.cloned.1.call-done) | copy-start | bytes 1572868
Sparse Core Ops, SparseCore 0:
  102.3 31.2 reduce-scatter.2
  137.1 22.5 all-gather.1
  401.0 30.9 reduce-scatter.4

commit v2 on v1

--- a/solution.py
+++ b/solution.py
@@ -28,20 +28,62 @@
     return out
 
 
-def mixer_kernel(
+def greet(barrier, ring, team):
+    me, mine = (lax.axis_index("sp"), lax.axis_index("tp"))
+    partner = me + 1 - 2 * (me % 2)
+    peers = [(lax.rem(me + apart, ring), mine) for apart in range(1, ring)]
+    for apart in range(1, team):
+        other = lax.rem(mine + apart, team)
+        peers += [(me, other), (partner, other)]
+    for at_sp, at_tp in peers:
+        pl.semaphore_signal(
+            barrier, inc=1, device_id={"sp": at_sp, "tp": at_tp}, device_id_type=MESH
+        )
+    return len(peers)
+
+
+def remote(src, dst, send, recv, at_sp, at_tp):
+    return pltpu.make_async_remote_copy(
+        src_ref=src,
+        dst_ref=dst,
+        send_sem=send,
+        recv_sem=recv,
+        device_id={"sp": at_sp, "tp": at_tp},
+        device_id_type=MESH,
+    )
+
+
+def diagonal(compact, copies, height, states):
+    tall = jnp.concatenate([compact] * copies, axis=0)
+    rows = lax.broadcasted_iota(jnp.int32, tall.shape, 0) // height
+    cols = lax.broadcasted_iota(jnp.int32, tall.shape, 1) // states
+    return jnp.where(rows == cols, tall, 0.0).astype(jnp.bfloat16)
+
+
+def entry_kernel(
     ring,
+    team,
     states,
     x_ref,
     damp_ref,
     abar_re_ref,
     abar_im_ref,
-    in_re_ref,
-    in_im_ref,
-    out_re_ref,
-    out_im_ref,
+    factor_re_ref,
+    factor_im_ref,
+    in_ref,
+    out_ref,
     skip_ref,
     w_out_ref,
-    proj_ref,
+    residual_ref,
+    gain_ref,
+    w_act_ref,
+    w_lin_ref,
+    w_down_ref,
+    stream_ref,
+    pair_ref,
+    act_ref,
+    lin_ref,
+    down_ref,
     growth,
     state_re,
     state_im,
@@ -49,15 +91,87 @@
     begin_im,
     outbox,
     inbox,
+    proj,
+    rs_in,
+    stage,
+    stage_down,
     send_sem,
     recv_sem,
+    rs_send,
+    rs_recv,
+    ag_send,
+    ag_recv,
+    hop_send,
+    hop_recv,
+    local_sem,
 ):
     bf16, f32 = (jnp.bfloat16, jnp.float32)
-    me = lax.axis_index("sp")
+    me, mine = (lax.axis_index("sp"), lax.axis_index("tp"))
     barrier = pltpu.get_barrier_semaphore()
-    for apart in range(1, ring):
-        peer = lax.rem(me + apart, ring)
-        pl.semaphore_signal(barrier, inc=1, device_id={"sp": peer}, device_id_type=MESH)
+    greeted = greet(barrier, ring, team)
+    parity = me % 2
+    partner = me + 1 - 2 * parity
+    circle = ring // 2
+    spot = me // 2
+    wide = stage.shape[2]
+    shift = w_act_ref.shape[1] - wide
+
+    def originals(side):
+        cut = pl.ds(pl.multiple_of(side * shift, 128), wide)
+        return [w_act_ref.at[:, cut], w_lin_ref.at[:, cut], w_down_ref.at[cut, :]]
+
+    gathered = [act_ref, lin_ref, down_ref]
+    keep = [stage.at[0], stage.at[1], stage_down]
+    loads = [
+        pltpu.make_async_copy(src, dst, local_sem.at[k])
+        for k, (src, dst) in enumerate(zip(originals(parity), keep))
+    ]
+    for load in loads:
+        load.start()
+    pl.semaphore_wait(barrier, greeted)
+    far, near = (circle // 2, (circle - 1) // 2)
+    hops = {"x": 0}
+    for name, count in (("or", far), ("ol", near), ("pl", far), ("pr", near)):
+        for hop in range(1, count + 1):
+            hops[name, hop] = len(hops)
+    hop_copies = {}
+
+    def send_blocks(key, sources, slot, target):
+        made = []
+        for k in range(3):
+            index = hops[key] * 3 + k
+            copy = remote(
+                sources[k],
+                gathered[k].at[slot],
+                hop_send.at[index],
+                hop_recv.at[index],
+                target,
+                mine,
+            )
+            copy.start()
+            made.append(copy)
+        hop_copies[key] = made
+
+    def hop_on(name, hop):
+        step = 1 if name[1] == "r" else circle - 1
+        target = ((spot + step) % circle) * 2 + parity
+        origin = ((spot + (hop - 1) * (circle - step)) % circle) * 2
+        if name[0] == "o":
+            slot = origin + parity
+            sources = originals(parity) if hop == 1 else [ref.at[slot] for ref in gathered]
+        else:
+            slot = origin + 1 - parity
+            sources = [ref.at[slot] for ref in gathered]
+        send_blocks((name, hop), sources, slot, target)
+
+    def landed(key):
+        for copy in hop_copies[key]:
+            copy.wait_recv()
+
+    send_blocks("x", originals(1 - parity), me, partner)
+    hop_on("or", 1)
+    if near:
+        hop_on("ol", 1)
     tokens = x_ref.shape[0]
     lanes = growth.shape[1]
     steps = tokens // SUB
@@ -79,20 +193,23 @@
     total = None
     for part in (high, middle, low):
         moved = jnp.dot(spread, part, preferred_element_type=f32).astype(bf16)
-        wide = jnp.dot(moved, pick, preferred_element_type=f32)
-        total = wide if total is None else total + wide
+        spanned = jnp.dot(moved, pick, preferred_element_type=f32)
+        total = spanned if total is None else total + spanned
     growth[...] = total
-    blocks = in_re_ref.shape[0]
-    width = in_re_ref.shape[1]
-    span = in_re_ref.shape[2]
+    height = in_ref.shape[1]
+    width = 128
+    per_block = width // height
+    span = per_block * states
+    blocks = groups // per_block
     for b in range(blocks):
         piece = x_perm[:, b * width : (b + 1) * width]
-        state_re[:, b * span : (b + 1) * span] = jnp.dot(
-            piece, in_re_ref[b], preferred_element_type=f32
-        )
-        state_im[:, b * span : (b + 1) * span] = jnp.dot(
-            piece, in_im_ref[b], preferred_element_type=f32
-        )
+        cut = slice(b * span, (b + 1) * span)
+        f_re, f_im = (factor_re_ref[:, cut], factor_im_ref[:, cut])
+        m_re, m_im = (in_ref[0, :, cut], in_ref[1, :, cut])
+        bbar_re = diagonal(f_re * m_re - f_im * m_im, per_block, height, states)
+        bbar_im = diagonal(f_re * m_im + f_im * m_re, per_block, height, states)
+        state_re[:, cut] = jnp.dot(piece, bbar_re, preferred_element_type=f32)
+        state_im[:, cut] = jnp.dot(piece, bbar_im, preferred_element_type=f32)
 
     def advance(start, keep, cut, re, im, a_re, a_im):
         row = pl.multiple_of(start * SUB, SUB)
@@ -138,16 +255,15 @@
     outbox[1:2, :] = at_im
     outbox[2:3, :] = all_re
     outbox[3:4, :] = all_im
-    pl.semaphore_wait(barrier, ring - 1)
     copies = []
     for apart in range(1, ring):
-        copy = pltpu.make_async_remote_copy(
-            src_ref=outbox,
-            dst_ref=inbox.at[apart],
-            send_sem=send_sem.at[apart],
-            recv_sem=recv_sem.at[apart],
-            device_id={"sp": lax.rem(me + apart, ring)},
-            device_id_type=MESH,
+        copy = remote(
+            outbox,
+            inbox.at[apart],
+            send_sem.at[apart],
+            recv_sem.at[apart],
+            lax.rem(me + apart, ring),
+            mine,
         )
         copy.start()
         copies.append(copy)
@@ -182,13 +298,22 @@
             return (re, im)
 
         lax.fori_loop(0, steps, body, (begin_re[:, cut], begin_im[:, cut]), unroll=4)
+
+    def across(state, compact):
+        return lax.dot_general(
+            state,
+            diagonal(compact, per_block, height, states),
+            (((1,), (1,)), ((), ())),
+            preferred_element_type=f32,
+        )
+
     pieces = []
     for b in range(blocks):
         cut = slice(b * span, (b + 1) * span)
         here = slice(b * width, (b + 1) * width)
         mixed = (
-            jnp.dot(state_re[:, cut].astype(bf16), out_re_ref[b], preferred_element_type=f32)
-            - jnp.dot(state_im[:, cut].astype(bf16), out_im_ref[b], preferred_element_type=f32)
+            across(state_re[:, cut].astype(bf16), out_ref[0, :, cut])
+            - across(state_im[:, cut].astype(bf16), out_ref[1, :, cut])
             + skip_ref[:, here] * x_perm[:, here].astype(f32)
         )
         pieces.append(jax.nn.gelu(mixed).astype(bf16))
@@ -200,30 +325,152 @@
 
     def project(k, _):
         there = pl.ds(pl.multiple_of(k * piece, piece), piece)
-        proj_ref[:, there] = jnp.dot(
+        proj[:, there] = jnp.dot(
             activated, w_out_ref[:, there], preferred_element_type=f32
         ).astype(bf16)
         return 0
 
     lax.fori_loop(0, columns // piece, project, 0)
-
-
-def block_diagonal(parts, per_block):
-    groups, rows, cols = parts.shape
-    blocks = groups // per_block
-    eye = jnp.eye(per_block, dtype=parts.dtype)
-    wide = (
-        parts.reshape(blocks, per_block, rows, 1, cols) * eye[None, :, None, :, None]
-    )
-    return wide.reshape(blocks, per_block * rows, per_block * cols).astype(jnp.bfloat16)
-
-
-def state_projection(
-    mixer_input, log_step, rate_real, rate_imag, damping, in_map, out_map, skip, w_out
+    share = tokens // team
+    sums = []
+    for apart in range(1, team):
+        other = lax.rem(mine + apart, team)
+        copy = remote(
+            proj.at[pl.ds(pl.multiple_of(other * share, share), share), :],
+            rs_in.at[apart],
+            rs_send.at[apart],
+            rs_recv.at[apart],
+            me,
+            other,
+        )
+        copy.start()
+        sums.append(copy)
+    stores = []
+    for k in range(3):
+        loads[k].wait()
+        store = pltpu.make_async_copy(keep[k], gathered[k].at[me], local_sem.at[3 + k])
+        store.start()
+        stores.append(store)
+    landed("x")
+    if near:
+        hop_on("pr", 1)
+    hop_on("pl", 1)
+    if far > 1:
+        landed(("or", 1))
+        hop_on("or", 2)
+    for copy in sums:
+        copy.wait()
+    total = proj[pl.ds(pl.multiple_of(mine * share, share), share), :].astype(f32)
+    for apart in range(1, team):
+        total = total + rs_in[apart].astype(f32)
+    stream = (residual_ref[...].astype(f32) + total).astype(bf16)
+    stream_ref[...] = stream
+    stream = stream.astype(f32)
+    scale = lax.rsqrt(jnp.mean(stream * stream, axis=-1, keepdims=True) + 1e-06)
+    place = pl.ds(pl.multiple_of(parity * tokens + mine * share, share), share)
+    pair_ref[place, :] = (stream * scale * gain_ref[...]).astype(bf16)
+    spread_copies = []
+    for k in range(2 * team - 1):
+        at_sp = partner if k < team else me
+        other = lax.rem(mine + (k if k < team else k - team + 1), team)
+        copy = remote(
+            pair_ref.at[place, :], pair_ref.at[place, :], ag_send.at[k], ag_recv.at[k], at_sp, other
+        )
+        copy.start()
+        spread_copies.append(copy)
+    if far > 1:
+        landed(("pl", 1))
+        hop_on("pl", 2)
+    if near > 1:
+        landed(("ol", 1))
+        hop_on("ol", 2)
+        landed(("pr", 1))
+        hop_on("pr", 2)
+    for hop in range(3, far + 1):
+        for name in ("or", "pl", "ol", "pr"):
+            if (name, hop) in hops:
+                landed((name, hop - 1))
+                hop_on(name, hop)
+    forwarded = {("or", h) for h in range(1, far)} | {("pl", h) for h in range(1, far)}
+    forwarded |= {("ol", h) for h in range(1, near)} | {("pr", h) for h in range(1, near)} | {"x"}
+    for copy in spread_copies:
+        copy.wait()
+    for key, made in hop_copies.items():
+        for copy in made:
+            copy.wait_send()
+            if key not in forwarded:
+                copy.wait_recv()
+    for store in stores:
+        store.wait()
+
+
+def exit_kernel(
+    ring, team, hidden_ref, down_ref, stream_ref, out_ref, outbox, inbox, send_sem, recv_sem
+):
+    f32 = jnp.float32
+    me, mine = (lax.axis_index("sp"), lax.axis_index("tp"))
+    partner = me + 1 - 2 * (me % 2)
+    barrier = pltpu.get_barrier_semaphore()
+    rows = out_ref.shape[0]
+    peers = [(partner, lax.rem(mine + apart, team)) for apart in range(team)]
+    peers += [(me, lax.rem(mine + apart, team)) for apart in range(1, team)]
+    for at_sp, at_tp in peers:
+        pl.semaphore_signal(
+            barrier, inc=1, device_id={"sp": at_sp, "tp": at_tp}, device_id_type=MESH
+        )
+    columns = down_ref.shape[1]
+    piece = min(512, columns)
+
+    def product(slot, at_sp, at_tp):
+        start = pl.multiple_of(((at_sp % 2) * team + at_tp) * rows, rows)
+        block = hidden_ref[pl.ds(start, rows), :]
+
+        def some(k, _):
+            there = pl.ds(pl.multiple_of(k * piece, piece), piece)
+            outbox[slot, :, there] = jnp.dot(
+                block, down_ref[:, there], preferred_element_type=f32
+            ).astype(jnp.bfloat16)
+            return 0
+
+        lax.fori_loop(0, columns // piece, some, 0)
+
+    copies = []
+    order = sorted(range(len(peers)), key=lambda k: (k >= team, -(k % team)))
+    for k in order:
+        product(k, *peers[k])
+        if not copies:
+            pl.semaphore_wait(barrier, len(peers))
+        copy = remote(outbox.at[k], inbox.at[k], send_sem.at[k], recv_sem.at[k], *peers[k])
+        copy.start()
+        copies.append(copy)
+    product(len(peers), me, mine)
+    for copy in copies:
+        copy.wait()
+    total = outbox[len(peers)].astype(f32)
+    for k in range(len(peers)):
+        total = total + inbox[k].astype(f32)
+    out_ref[...] = (stream_ref[...].astype(f32) + total).astype(jnp.bfloat16)
+
+
+def enter_layer(
+    mixer_input,
+    residual,
+    log_step,
+    rate_real,
+    rate_imag,
+    damping,
+    in_map,
+    out_map,
+    skip,
+    w_out,
+    norm_gain,
+    w_act,
+    w_lin,
+    w_down,
+    wide,
 ):
     tokens_here, channels = mixer_input.shape
     groups_here, states = rate_real.shape
-    group_width = channels // groups_here
     step_size = jnp.exp(log_step)[:, None]
     log_rate = rate_real * step_size
     angle_step = rate_imag * step_size
@@ -234,18 +481,26 @@
     minus_one = abar_re - 1.0
     factor_re = (minus_one * rate_real + abar_im * rate_imag) / denominator
     factor_im = (abar_im * rate_real - minus_one * rate_imag) / denominator
-    bbar_re = factor_re[..., None] * in_map[0] - factor_im[..., None] * in_map[1]
-    bbar_im = factor_re[..., None] * in_map[1] + factor_im[..., None] * in_map[0]
-    per_block = 128 // group_width
     lanes = groups_here * states
-    ring = lax.axis_size("sp")
+    ring, team = (lax.axis_size("sp"), lax.axis_size("tp"))
+    width = w_out.shape[1]
     vmem = pl.BlockSpec(memory_space=pltpu.VMEM)
-    f32 = jnp.float32
+    anywhere = pl.BlockSpec(memory_space=pl.ANY)
+    f32, bf16 = (jnp.float32, jnp.bfloat16)
+    group_width = channels // groups_here
+    dma = pltpu.SemaphoreType.DMA
+    hop_count = 3 * (1 + 2 * (ring // 2 - 1))
     return pl.pallas_call(
-        functools.partial(mixer_kernel, ring, states),
-        out_shape=jax.ShapeDtypeStruct((tokens_here, w_out.shape[1]), jnp.bfloat16),
-        in_specs=[vmem] * 10,
-        out_specs=vmem,
+        functools.partial(entry_kernel, ring, team, states),
+        out_shape=(
+            jax.ShapeDtypeStruct((tokens_here // team, width), bf16),
+            jax.ShapeDtypeStruct((2 * tokens_here, width), bf16),
+            jax.ShapeDtypeStruct((ring, w_act.shape[0], wide), bf16),
+            jax.ShapeDtypeStruct((ring, w_lin.shape[0], wide), bf16),
+            jax.ShapeDtypeStruct((ring, wide, w_down.shape[1]), bf16),
+        ),
+        in_specs=[vmem] * 12 + [anywhere] * 3,
+        out_specs=(vmem, vmem, anywhere, anywhere, anywhere),
         scratch_shapes=[
             pltpu.VMEM((tokens_here, lanes), f32),
             pltpu.VMEM((tokens_here, lanes), f32),
@@ -254,8 +509,19 @@
             pltpu.VMEM((SUB, lanes), f32),
             pltpu.VMEM((4, lanes), f32),
             pltpu.VMEM((ring, 4, lanes), f32),
-            pltpu.SemaphoreType.DMA((ring,)),
-            pltpu.SemaphoreType.DMA((ring,)),
+            pltpu.VMEM((tokens_here, width), bf16),
+            pltpu.VMEM((team, tokens_here // team, width), bf16),
+            pltpu.VMEM((2, w_act.shape[0], wide), bf16),
+            pltpu.VMEM((wide, w_down.shape[1]), bf16),
+            dma((ring,)),
+            dma((ring,)),
+            dma((team,)),
+            dma((team,)),
+            dma((2 * team - 1,)),
+            dma((2 * team - 1,)),
+            dma((hop_count,)),
+            dma((hop_count,)),
+            dma((6,)),
         ],
         compiler_params=pltpu.CompilerParams(
             collective_id=0, has_side_effects=True, vmem_limit_bytes=56 * 1024 * 1024
@@ -263,41 +529,55 @@
         cost_estimate=pl.CostEstimate(
             flops=20_000_000_000, bytes_accessed=8_000_000, transcendentals=0
         ),
-        name="state_projection",
+        name="enter_layer",
     )(
         mixer_input,
         damping,
         abar_re.reshape(1, lanes),
         abar_im.reshape(1, lanes),
-        block_diagonal(jnp.swapaxes(bbar_re, 1, 2), per_block),
-        block_diagonal(jnp.swapaxes(bbar_im, 1, 2), per_block),
-        block_diagonal(jnp.swapaxes(out_map[0], 1, 2), per_block),
-        block_diagonal(jnp.swapaxes(out_map[1], 1, 2), per_block),
+        factor_re.reshape(1, lanes),
+        factor_im.reshape(1, lanes),
+        jnp.transpose(in_map, (0, 3, 1, 2)).reshape(2, group_width, lanes),
+        jnp.transpose(out_map, (0, 2, 1, 3)).reshape(2, group_width, lanes),
         skip.reshape(1, channels),
         w_out,
+        residual,
+        norm_gain.reshape(1, width),
+        w_act,
+        w_lin,
+        w_down,
     )
 
 
-def from_partner(block, axis, apart):
-    count = lax.axis_size(axis)
-    route = []
-    for low in range(count):
-        high = low | 1 << apart
-        if high != low and high < count:
-            route += [(low, high), (high, low)]
-    return lax.ppermute(block, axis, route)
+def leave_layer(hidden, down, stream):
+    ring, team = (lax.axis_size("sp"), lax.axis_size("tp"))
+    rows, width = stream.shape
+    vmem = pl.BlockSpec(memory_space=pltpu.VMEM)
+    return pl.pallas_call(
+        functools.partial(exit_kernel, ring, team),
+        out_shape=jax.ShapeDtypeStruct((rows, width), jnp.bfloat16),
+        in_specs=[vmem] * 3,
+        out_specs=vmem,
+        scratch_shapes=[
+            pltpu.VMEM((2 * team, rows, width), jnp.bfloat16),
+            pltpu.VMEM((2 * team - 1, rows, width), jnp.bfloat16),
+            pltpu.SemaphoreType.DMA((2 * team - 1,)),
+            pltpu.SemaphoreType.DMA((2 * team - 1,)),
+        ],
+        compiler_params=pltpu.CompilerParams(
+            collective_id=1, has_side_effects=True, vmem_limit_bytes=48 * 1024 * 1024
+        ),
+        cost_estimate=pl.CostEstimate(
+            flops=20_000_000_000, bytes_accessed=8_000_000, transcendentals=0
+        ),
+        name="leave_layer",
+    )(hidden, down, stream)
 
 
 def from_behind(value, axis, steps):
     count = lax.axis_size(axis)
     initial, last = (max(0, -steps), min(count, count - steps))
     return lax.ppermute(value, axis, [(source, source + steps) for source in range(initial, last)])
-
-
-def normalize(stream, norm_gain):
-    stream_f = stream.astype(jnp.float32)
-    scale = lax.rsqrt(jnp.mean(stream_f * stream_f, axis=-1, keepdims=True) + 1e-06)
-    return (stream_f * scale * norm_gain).astype(jnp.bfloat16)
 
 
 def causal_conv(act_pre, lin_pre, previous, taps):
@@ -331,37 +611,28 @@
 ):
     tokens_here = mixer_input.shape[0]
     hidden_here = w_act.shape[1]
-    partial_projection = state_projection(
-        mixer_input, log_step, rate_real, rate_imag, damping, in_map, out_map, skip, w_out
+    wide = -(-hidden_here // 256) * 128
+    parity = lax.axis_index("sp") % 2
+    stream, normed_pair, act_all, lin_all, down_all = enter_layer(
+        mixer_input,
+        residual,
+        log_step,
+        rate_real,
+        rate_imag,
+        damping,
+        in_map,
+        out_map,
+        skip,
+        w_out,
+        norm_gain,
+        w_act,
+        w_lin,
+        w_down,
+        wide,
     )
-    projected = lax.psum_scatter(
-        partial_projection,
-        "tp",
-        scatter_dimension=0,
-        tiled=True,
-    ).astype(jnp.float32)
-    stream = (residual.astype(jnp.float32) + projected).astype(jnp.bfloat16)
-    normed_all = lax.all_gather(normalize(stream, norm_gain), "tp", axis=0, tiled=True)
-    parity = lax.axis_index("sp") % 2
-    half = hidden_here // 2
-    copies = lax.axis_size("sp") // 2
-
-    def outgoing_rows(weight):
-        paired = jnp.concatenate([weight[:, :half], weight[:, half:]], axis=0)
-        return jnp.tile(paired, (copies, 1))
-
-    act_half, lin_half = (
-        lax.all_to_all(outgoing_rows(w_act), "sp", split_axis=0, concat_axis=0, tiled=True),
-        lax.all_to_all(outgoing_rows(w_lin), "sp", split_axis=0, concat_axis=0, tiled=True),
-    )
-    paired_down = jnp.concatenate([w_down[:half], w_down[half:]], axis=1)
-    down_half = lax.all_to_all(
-        jnp.tile(paired_down, (1, copies)), "sp", split_axis=1, concat_axis=1, tiled=True
-    )
-    partner = from_partner(normed_all, "sp", 0)
-    first = jnp.where(parity == 0, normed_all, partner)
-    second = jnp.where(parity == 0, partner, normed_all)
-    normed_pair = jnp.concatenate([first, second], axis=0)
+    act_half = act_all.reshape(-1, wide)
+    lin_half = lin_all.reshape(-1, wide)
+    down_half = jnp.transpose(down_all, (1, 0, 2)).reshape(wide, -1)
     act_pre = jnp.dot(normed_pair, act_half, preferred_element_type=jnp.float32).astype(
         jnp.bfloat16
     )
@@ -370,16 +641,11 @@
     )
     edge = 2 * tokens_here - (CONV - 1)
     previous = from_behind((act_pre[edge:], lin_pre[edge:]), "sp", 2)
-    taps = lax.dynamic_slice_in_dim(conv_taps, parity * half, half, 2)
+    taps = lax.dynamic_slice_in_dim(conv_taps, parity * (hidden_here - wide), wide, 2)
     hidden = causal_conv(act_pre, lin_pre, previous, taps)
-    partial_value = jnp.dot(hidden, down_half, preferred_element_type=jnp.float32)
-    mine = lax.dynamic_slice_in_dim(partial_value, parity * tokens_here, tokens_here, 0)
-    other = lax.dynamic_slice_in_dim(partial_value, (1 - parity) * tokens_here, tokens_here, 0)
-    block_total = mine + from_partner(other, "sp", 0)
-    channel_sum = lax.psum_scatter(
-        block_total.astype(jnp.bfloat16), "tp", scatter_dimension=0, tiled=True
-    ).astype(jnp.float32)
-    return (stream.astype(jnp.float32) + channel_sum).astype(jnp.bfloat16)
+    doubled = parity * (2 * wide - hidden_here)
+    hidden = jnp.where(jnp.arange(wide)[None, :] >= doubled, hidden, jnp.zeros_like(hidden))
+    return leave_layer(hidden, down_half, stream)
 
 
 def solution(mesh):

time: 442 us -> 265 us (0.60)
  waiting for transfers between devices: 241 us -> 0.01 us
  Pallas kernels: 42.8 us -> 229 us
  local copies, waits for them, and re-layouts: 83.1 us -> 13.7 us
  starting transfers between devices: 25.7 us -> 5.51 us
  other arithmetic: 21.2 us -> 5.77 us
  between operations: 13.4 us -> 0.25 us
    pallas_call x1 -> x2, Pallas kernels: 42.8 us -> 229 us  [the longest x1 176 us: enter_layer(): pl.pallas_call(functools.partial(entry_kernel, ring, team, states), out_s...]
    ppermute x2 -> x0, waiting for transfers between devices: 102 us -> none  [from_partner(): return lax.ppermute(block, axis, route)]
    all_to_all x3 -> x0, waiting for transfers between devices: 96.5 us -> none  [the longest x1 56.7 us: per_device(): lax.all_to_all(jnp.tile(paired_down, (1, copies)), 'sp', split_axis=1, co...]
    reduce_scatter x2 -> x0, waiting for transfers between devices: 39.8 us -> none  [the longest x1 31.1 us: per_device(): lax.psum_scatter(block_total.astype(jnp.bfloat16), 'tp', scatter_dimensio...]
    all_to_all x9 -> x0, local copies, waits for them, and re-layouts: 34.3 us -> none  [the longest x3 13.6 us: per_device(): lax.all_to_all(outgoing_rows(w_lin), 'sp', split_axis=0, concat_axis=0, t...]
    mul x17 -> x0, local copies, waits for them, and re-layouts: 25.7 us -> none  [block_diagonal(): parts.reshape(blocks, per_block, rows, 1, cols)]
    all_to_all x3 -> x0, starting transfers between devices: 16.7 us -> none  [the longest x1 7.41 us: per_device(): lax.all_to_all(outgoing_rows(w_act), 'sp', split_axis=0, concat_axis=0, t...]
    convert_element_type x6 -> x0, other arithmetic: 13.8 us -> none  [the longest x1 5.44 us: per_device(): block_total.astype(jnp.bfloat16)]
  transfers between devices with their start and end apart: 10 -> 2, of which waited for: 7 -> 0; matrix products, arithmetic and copies ran while one was open for 16% -> 3% of each run, Pallas kernels for 10% -> 0%
where the time goes in v2:
time: 265 us
  Pallas kernels  229 us (86%)
  local copies, waits for them, and re-layouts  13.7 us (5%)
  matrix products  10.1 us (4%)
  other arithmetic  5.77 us (2%)
  starting transfers between devices  5.51 us (2%)
    pallas_call x1, Pallas kernels, enter_layer(): pl.pallas_call(functools.partial(entry_kernel, ring, team, states), out_s...  176 us
    pallas_call x1, Pallas kernels, leave_layer(): pl.pallas_call(functools.partial(exit_kernel, ring, team), out_shape=jax....  53.4 us
    dot_general x1, matrix products, per_device(): jnp.dot(normed_pair, act_half, preferred_element_type=jnp.float32)  6.7 us
    ppermute x2, starting transfers between devices, from_behind(): lax.ppermute(value, axis, [(source, source + steps) for source in range(i...  5.51 us
  transfers between devices with their start and end apart: 2, of which 0 were waited for; matrix products, arithmetic and copies ran while one was open for 3% of the time, Pallas kernels for 0%

profile of v2, /device:TPU:0, one launch (start us, length us, event | category | flops | bytes accessed | tf_op | source)
XLA Modules:
  0.0 264.8 jit_solution(7555318169047403363)
XLA Ops:
  0.0 0.7 exp.10
  0.7 0.9 subtract_divide_fusion
  1.6 0.7 reshape.48.factor_im_ref
  2.2 0.7 reshape.46.abar_im_ref
  2.9 0.7 reshape.45.abar_re_ref
  3.6 0.7 reshape.47.factor_re_ref
  4.2 1.7 copy.18.damp_ref
  5.9 1.2 copy.16
  7.1 0.9 reshape.49.in_ref
  8.0 1.2 copy.17
  9.2 0.9 reshape.50.out_ref
  10.1 176.1 %enter_layer.1 = (bf16[128,2048]{1,0:T(8,128)(2,1)}, bf16[1024,2048]{1,0:T(8,128)(2,1)}, bf16[8,256,768]{2,1,0:T(8,128)(2,1)}, bf16[8,256,768]{2,1,0:T(8,128)(2,1)}, bf16[8,768,256]{2,1,0:T(8,128)(2,1)}) custom-call(bf16[512,512]{1,0:T(8,128)(2,1)} %x_ref.1, f32[512,32]{1,0:T(8,128)} %copy.18.damp_ref, f32[1,2048]{1,0:T(1,128)} %reshape.45.abar_re_ref, ...), custom_call_target="tpu_custom_call" | custom-call | flops 20000000000 | bytes 8000000 | tf_op jit(solution)/shard_map/enter_layer/pallas_call | solution.py:493
  186.2 0.0 copy-start.5
  186.2 0.0 copy-start.6
  186.2 6.7 %convolution_convert_fusion.1 = bf16[1024,768]{1,0:T(8,128)(2,1)S(1)} fusion(bf16[1024,2048]{1,0:T(8,128)(2,1)} %get-tuple-element.10, bf16[2048,768]{1,0:T(8,128)(2,1)} %bitcast.24), kind=kOutput, calls=%fused_computation.13 | convolution fusion | flops 3222011904 | bytes 8912896 | tf_op jit(solution)/shard_map/dot_general | solution.py:636
  192.9 0.0 copy-start.1
  192.9 2.4 collective-permute-start
  195.3 3.4 %convolution_convert_fusion = bf16[1024,768]{1,0:T(8,128)(2,1)S(1)} fusion(bf16[1024,2048]{1,0:T(8,128)(2,1)S(1)} %copy-done.6, bf16[2048,768]{1,0:T(8,128)(2,1)S(1)} %bitcast.23), kind=kOutput, calls=%fused_computation.12 | convolution fusion | flops 3222011904 | bytes 8912896 | tf_op jit(solution)/shard_map/dot_general | solution.py:639
  198.8 0.0 copy-done.1
  198.8 0.0 copy-start.3
  198.8 1.2 copy-done.3
  200.0 3.1 %collective-permute-start.1 = (bf16[2,768]{1,0:T(2,128)(2,1)S(1)}, bf16[2,768]{1,0:T(2,128)(2,1)S(1)}, u32[]{:S(2)}, u32[]{:S(2)}) collective-permute-start(bf16[2,768]{1,0:T(2,128)(2,1)S(1)} %slice.60), channel_id=1, source_target_pairs={{0,8},{4,12},{8,16},{12,20},{16,24},{20,28},{1,9},{5,13},{9,17},{1... | collective-permute-start | bytes 9224 | tf_op jit(solution)/shard_map/ppermute | solution.py:580
  203.2 0.0 copy-start.4
  203.2 2.3 copy.20
  205.6 0.1 dynamic-slice_reduce_fusion.5
  205.7 0.0 collective-permute-done.1
  205.7 1.8 maximum_convert_fusion.1
  207.5 0.0 collective-permute-done
  207.5 0.3 maximum_convert_fusion
  207.8 2.7 %broadcast_select_fusion.hidden_ref = bf16[1024,768]{1,0:T(8,128)(2,1)S(1)} fusion(pred[768]{0:T(1024)(128)(4,1)S(1)} %iota_compare_fusion, f32[1026,768]{1,0:T(8,128)S(1)} %maximum_convert_fusion.1, f32[768]{0:T(1024)S(1)} %get-tuple-element.20, f32[768]{0:T(1024)S(1)} %get-tuple-element.16, f32[768]{0:T(1024)S(1)} %get-tuple-element.17, ...), kind=kLoop, calls=%fused_computation.16 | loop fusion | flops 13369344 | bytes 20466432 | tf_op jit(solution)/shard_map/jit(_where)/select_n | solution.py:647
  210.6 53.4 %leave_layer.1 = bf16[128,2048]{1,0:T(8,128)(2,1)S(1)} custom-call(bf16[1024,768]{1,0:T(8,128)(2,1)S(1)} %broadcast_select_fusion.hidden_ref, bf16[768,2048]{1,0:T(8,128)(2,1)S(1)} %bitcast.17, bf16[128,2048]{1,0:T(8,128)(2,1)S(1)} %copy-done), custom_call_target="tpu_custom_call" | custom-call | flops 20000000000 | bytes 8000000 | tf_op jit(solution)/shard_map/leave_layer/pallas_call | solution.py:556
  264.0 0.8 copy.22
  (10 shorter events, 0.0 us)
Async XLA Ops:
  186.2 9.1 %copy-start.5 = (bf16[8,256,768]{2,1,0:T(8,128)(2,1)S(1)}, bf16[8,256,768]{2,1,0:T(8,128)(2,1)}, u32[]{:S(2)}) copy-start(bf16[8,256,768]{2,1,0:T(8,128)(2,1)} %get-tuple-element.12) | copy-start | bytes 9437188
  186.2 9.1 %copy-start.6 = (bf16[1024,2048]{1,0:T(8,128)(2,1)S(1)}, bf16[1024,2048]{1,0:T(8,128)(2,1)}, u32[]{:S(2)}) copy-start(bf16[1024,2048]{1,0:T(8,128)(2,1)} %get-tuple-element.10) | copy-start | bytes 12582916
  192.9 5.8 %copy-start.1 = (bf16[1024,768]{1,0:T(8,128)(2,1)}, bf16[1024,768]{1,0:T(8,128)(2,1)S(1)}, u32[]{:S(2)}) copy-start(bf16[1024,768]{1,0:T(8,128)(2,1)S(1)} %convolution_convert_fusion.1) | copy-start | bytes 4718596
  192.9 14.5 %collective-permute-start = (bf16[2,768]{1,0:T(2,128)(2,1)S(1)}, bf16[2,768]{1,0:T(2,128)(2,1)S(1)}, u32[]{:S(2)}, u32[]{:S(2)}) collective-permute-start(bf16[2,768]{1,0:T(2,128)(2,1)S(1)} %slice.56), channel_id=1, source_target_pairs={{0,8},{4,12},{8,16},{12,20},{16,24},{20,28},{1,9},{5,13},{9,17},{1... | collective-permute-start | bytes 9224 | tf_op jit(solution)/shard_map/ppermute | solution.py:580
  198.8 1.2 copy-start.3
  200.0 5.7 %collective-permute-start.1 = (bf16[2,768]{1,0:T(2,128)(2,1)S(1)}, bf16[2,768]{1,0:T(2,128)(2,1)S(1)}, u32[]{:S(2)}, u32[]{:S(2)}) collective-permute-start(bf16[2,768]{1,0:T(2,128)(2,1)S(1)} %slice.60), channel_id=1, source_target_pairs={{0,8},{4,12},{8,16},{12,20},{16,24},{20,28},{1,9},{5,13},{9,17},{1... | collective-permute-start | bytes 9224 | tf_op jit(solution)/shard_map/ppermute | solution.py:580
  203.2 2.3 copy-start.4
  205.5 2.0 copy-start.2
  207.8 2.8 %copy-start = (bf16[128,2048]{1,0:T(8,128)(2,1)S(1)}, bf16[128,2048]{1,0:T(8,128)(2,1)}, u32[]{:S(2)}) copy-start(bf16[128,2048]{1,0:T(8,128)(2,1)} %get-tuple-element.14.stream_ref) | copy-start | bytes 1572868

commit v3 on v2

--- a/solution.py
+++ b/solution.py
@@ -307,6 +307,13 @@
             preferred_element_type=f32,
         )
 
+    landed("x")
+    if near:
+        hop_on("pr", 1)
+    hop_on("pl", 1)
+    if far > 1:
+        landed(("or", 1))
+        hop_on("or", 2)
     pieces = []
     for b in range(blocks):
         cut = slice(b * span, (b + 1) * span)
@@ -351,13 +358,6 @@
         store = pltpu.make_async_copy(keep[k], gathered[k].at[me], local_sem.at[3 + k])
         store.start()
         stores.append(store)
-    landed("x")
-    if near:
-        hop_on("pr", 1)
-    hop_on("pl", 1)
-    if far > 1:
-        landed(("or", 1))
-        hop_on("or", 2)
     for copy in sums:
         copy.wait()
     total = proj[pl.ds(pl.multiple_of(mine * share, share), share), :].astype(f32)
@@ -369,15 +369,28 @@
     scale = lax.rsqrt(jnp.mean(stream * stream, axis=-1, keepdims=True) + 1e-06)
     place = pl.ds(pl.multiple_of(parity * tokens + mine * share, share), share)
     pair_ref[place, :] = (stream * scale * gain_ref[...]).astype(bf16)
+    sibling = mine + 1 - 2 * (mine % 2)
     spread_copies = []
-    for k in range(2 * team - 1):
-        at_sp = partner if k < team else me
-        other = lax.rem(mine + (k if k < team else k - team + 1), team)
-        copy = remote(
-            pair_ref.at[place, :], pair_ref.at[place, :], ag_send.at[k], ag_recv.at[k], at_sp, other
-        )
+
+    def send_rows(owner_sp, owner_tp, at_sp, at_tp):
+        k = len(spread_copies)
+        start = (owner_sp % 2) * tokens + owner_tp * share
+        here = pair_ref.at[pl.ds(pl.multiple_of(start, share), share), :]
+        copy = remote(here, here, ag_send.at[k], ag_recv.at[k], at_sp, at_tp)
         copy.start()
         spread_copies.append(copy)
+
+    send_rows(me, mine, partner, mine)
+    owners = [(partner, mine)]
+    for apart in range(2, team, 2):
+        to_tp, from_tp = (lax.rem(mine + apart, team), lax.rem(mine + team - apart, team))
+        for side in (me, partner):
+            send_rows(me, mine, side, to_tp)
+            owners.append((side, from_tp))
+    send_rows(me, mine, me, sibling)
+    for k, owner in enumerate(owners):
+        spread_copies[k].wait_recv()
+        send_rows(*owner, me, sibling)
     if far > 1:
         landed(("pl", 1))
         hop_on("pl", 2)
@@ -393,8 +406,10 @@
                 hop_on(name, hop)
     forwarded = {("or", h) for h in range(1, far)} | {("pl", h) for h in range(1, far)}
     forwarded |= {("ol", h) for h in range(1, near)} | {("pr", h) for h in range(1, near)} | {"x"}
-    for copy in spread_copies:
-        copy.wait()
+    for k, copy in enumerate(spread_copies):
+        copy.wait_send()
+        if k >= len(owners):
+            copy.wait_recv()
     for key, made in hop_copies.items():
         for copy in made:
             copy.wait_send()

time: 265 us -> 262 us (0.989)
  Pallas kernels: 229 us -> 226 us
    pallas_call x1, Pallas kernels: 176 us -> 173 us  [enter_layer(): pl.pallas_call(functools.partial(entry_kernel, ring, team, states), out_s...]
where the time goes in v3:
time: 262 us; the launch traced here: 261 us
  Pallas kernels  226 us (86%)
  local copies, waits for them, and re-layouts  13.7 us (5%)
  matrix products  10.1 us (4%)
  other arithmetic  5.77 us (2%)
  starting transfers between devices  5.4 us (2%)
    pallas_call x1, Pallas kernels, enter_layer(): pl.pallas_call(functools.partial(entry_kernel, ring, team, states), out_s...  173 us
    pallas_call x1, Pallas kernels, leave_layer(): pl.pallas_call(functools.partial(exit_kernel, ring, team), out_shape=jax....  53.4 us
    dot_general x1, matrix products, per_device(): jnp.dot(normed_pair, act_half, preferred_element_type=jnp.float32)  6.71 us
    ppermute x2, starting transfers between devices, from_behind(): lax.ppermute(value, axis, [(source, source + steps) for source in range(i...  5.4 us
  transfers between devices with their start and end apart: 2, of which 0 were waited for; matrix products, arithmetic and copies ran while one was open for 3% of the time, Pallas kernels for 0%

profile of v3, /device:TPU:0, one launch (start us, length us, event | category | flops | bytes accessed | tf_op | source)
XLA Modules:
  0.0 261.4 jit_solution(1646669805645756996)
XLA Ops:
  0.0 0.7 exp.10
  0.7 0.9 subtract_divide_fusion
  1.6 0.7 reshape.48.factor_im_ref
  2.2 0.7 reshape.46.abar_im_ref
  2.9 0.7 reshape.45.abar_re_ref
  3.6 0.7 reshape.47.factor_re_ref
  4.2 1.7 copy.18.damp_ref
  5.9 1.2 copy.16
  7.1 0.9 reshape.49.in_ref
  8.0 1.2 copy.17
  9.2 0.9 reshape.50.out_ref
  10.1 172.8 %enter_layer.1 = (bf16[128,2048]{1,0:T(8,128)(2,1)}, bf16[1024,2048]{1,0:T(8,128)(2,1)}, bf16[8,256,768]{2,1,0:T(8,128)(2,1)}, bf16[8,256,768]{2,1,0:T(8,128)(2,1)}, bf16[8,768,256]{2,1,0:T(8,128)(2,1)}) custom-call(bf16[512,512]{1,0:T(8,128)(2,1)} %x_ref.1, f32[512,32]{1,0:T(8,128)} %copy.18.damp_ref, f32[1,2048]{1,0:T(1,128)} %reshape.45.abar_re_ref, ...), custom_call_target="tpu_custom_call" | custom-call | flops 20000000000 | bytes 8000000 | tf_op jit(solution)/shard_map/enter_layer/pallas_call | solution.py:508
  182.9 0.0 copy-start.5
  182.9 0.0 copy-start.6
  182.9 6.7 %convolution_convert_fusion.1 = bf16[1024,768]{1,0:T(8,128)(2,1)S(1)} fusion(bf16[1024,2048]{1,0:T(8,128)(2,1)} %get-tuple-element.10, bf16[2048,768]{1,0:T(8,128)(2,1)} %bitcast.24), kind=kOutput, calls=%fused_computation.13 | convolution fusion | flops 3222011904 | bytes 8912896 | tf_op jit(solution)/shard_map/dot_general | solution.py:651
  189.6 2.4 collective-permute-start
  192.1 3.4 %convolution_convert_fusion = bf16[1024,768]{1,0:T(8,128)(2,1)S(1)} fusion(bf16[1024,2048]{1,0:T(8,128)(2,1)S(1)} %copy-done.6, bf16[2048,768]{1,0:T(8,128)(2,1)S(1)} %bitcast.23), kind=kOutput, calls=%fused_computation.12 | convolution fusion | flops 3222011904 | bytes 8912896 | tf_op jit(solution)/shard_map/dot_general | solution.py:654
  195.6 1.2 copy-done.3
  196.8 3.0 %collective-permute-start.1 = (bf16[2,768]{1,0:T(2,128)(2,1)S(1)}, bf16[2,768]{1,0:T(2,128)(2,1)S(1)}, u32[]{:S(2)}, u32[]{:S(2)}) collective-permute-start(bf16[2,768]{1,0:T(2,128)(2,1)S(1)} %slice.60), channel_id=1, source_target_pairs={{0,8},{4,12},{8,16},{12,20},{16,24},{20,28},{1,9},{5,13},{9,17},{1... | collective-permute-start | bytes 9224 | tf_op jit(solution)/shard_map/ppermute | solution.py:595
  199.8 0.0 copy-start.4
  199.8 2.3 copy.20
  202.1 0.1 dynamic-slice_reduce_fusion.5
  202.3 0.0 collective-permute-done.1
  202.3 1.8 maximum_convert_fusion.1
  204.1 0.0 collective-permute-done
  204.1 0.0 copy-done.2
  204.1 0.3 maximum_convert_fusion
  204.4 0.0 copy-start
  204.4 2.7 %broadcast_select_fusion.hidden_ref = bf16[1024,768]{1,0:T(8,128)(2,1)S(1)} fusion(pred[768]{0:T(1024)(128)(4,1)S(1)} %iota_compare_fusion, f32[1026,768]{1,0:T(8,128)S(1)} %maximum_convert_fusion.1, f32[768]{0:T(1024)S(1)} %get-tuple-element.20, f32[768]{0:T(1024)S(1)} %get-tuple-element.16, f32[768]{0:T(1024)S(1)} %get-tuple-element.17, ...), kind=kLoop, calls=%fused_computation.16 | loop fusion | flops 13369344 | bytes 20466432 | tf_op jit(solution)/shard_map/jit(_where)/select_n | solution.py:662
  207.2 0.0 copy-done
  207.2 53.4 %leave_layer.1 = bf16[128,2048]{1,0:T(8,128)(2,1)S(1)} custom-call(bf16[1024,768]{1,0:T(8,128)(2,1)S(1)} %broadcast_select_fusion.hidden_ref, bf16[768,2048]{1,0:T(8,128)(2,1)S(1)} %bitcast.17, bf16[128,2048]{1,0:T(8,128)(2,1)S(1)} %copy-done), custom_call_target="tpu_custom_call" | custom-call | flops 20000000000 | bytes 8000000 | tf_op jit(solution)/shard_map/leave_layer/pallas_call | solution.py:571
  260.6 0.8 copy.22
  (10 shorter events, 0.0 us)
Async XLA Ops:
  182.9 9.2 %copy-start.5 = (bf16[8,256,768]{2,1,0:T(8,128)(2,1)S(1)}, bf16[8,256,768]{2,1,0:T(8,128)(2,1)}, u32[]{:S(2)}) copy-start(bf16[8,256,768]{2,1,0:T(8,128)(2,1)} %get-tuple-element.12) | copy-start | bytes 9437188
  182.9 9.2 %copy-start.6 = (bf16[1024,2048]{1,0:T(8,128)(2,1)S(1)}, bf16[1024,2048]{1,0:T(8,128)(2,1)}, u32[]{:S(2)}) copy-start(bf16[1024,2048]{1,0:T(8,128)(2,1)} %get-tuple-element.10) | copy-start | bytes 12582916
  189.6 5.9 %copy-start.1 = (bf16[1024,768]{1,0:T(8,128)(2,1)}, bf16[1024,768]{1,0:T(8,128)(2,1)S(1)}, u32[]{:S(2)}) copy-start(bf16[1024,768]{1,0:T(8,128)(2,1)S(1)} %convolution_convert_fusion.1) | copy-start | bytes 4718596
  189.6 14.4 %collective-permute-start = (bf16[2,768]{1,0:T(2,128)(2,1)S(1)}, bf16[2,768]{1,0:T(2,128)(2,1)S(1)}, u32[]{:S(2)}, u32[]{:S(2)}) collective-permute-start(bf16[2,768]{1,0:T(2,128)(2,1)S(1)} %slice.56), channel_id=1, source_target_pairs={{0,8},{4,12},{8,16},{12,20},{16,24},{20,28},{1,9},{5,13},{9,17},{1... | collective-permute-start | bytes 9224 | tf_op jit(solution)/shard_map/ppermute | solution.py:595
  195.5 1.2 copy-start.3
  196.8 5.5 %collective-permute-start.1 = (bf16[2,768]{1,0:T(2,128)(2,1)S(1)}, bf16[2,768]{1,0:T(2,128)(2,1)S(1)}, u32[]{:S(2)}, u32[]{:S(2)}) collective-permute-start(bf16[2,768]{1,0:T(2,128)(2,1)S(1)} %slice.60), channel_id=1, source_target_pairs={{0,8},{4,12},{8,16},{12,20},{16,24},{20,28},{1,9},{5,13},{9,17},{1... | collective-permute-start | bytes 9224 | tf_op jit(solution)/shard_map/ppermute | solution.py:595
  199.8 2.3 copy-start.4
  202.1 2.0 copy-start.2
  204.4 2.8 %copy-start = (bf16[128,2048]{1,0:T(8,128)(2,1)S(1)}, bf16[128,2048]{1,0:T(8,128)(2,1)}, u32[]{:S(2)}) copy-start(bf16[128,2048]{1,0:T(8,128)(2,1)} %get-tuple-element.14.stream_ref) | copy-start | bytes 1572868
